TPU v7x, 512 devices: a whole 4x8x8 slice. The times are simulated.
512 devices in a mesh: sp: 64 (over z, y), tp: 8 (over x, core).
Axes of the slice: x: 4, y: 8, z: 8, core: 2. Of those that a mesh axis runs over, the one named last changes fastest.
Arguments:
- residual: bfloat16 [12288, 2048], P(('sp', 'tp')), may hold values from -6 to 6
- queries_narrow: bfloat16 [12288, 512], P('sp', 'tp'), may hold values from -24 to 24
- keys_narrow: bfloat16 [12288, 512], P('sp', 'tp'), may hold values from -24 to 24
- values_narrow: bfloat16 [12288, 512], P('sp', 'tp'), may hold values from -6 to 6
- queries_broad: bfloat16 [12288, 512], P('sp', 'tp'), may hold values from -24 to 24
- keys_broad: bfloat16 [12288, 512], P('sp', 'tp'), may hold values from -24 to 24
- values_broad: bfloat16 [12288, 512], P('sp', 'tp'), may hold values from -6 to 6
- gates_narrow: float32 [12288, 16], P('sp', 'tp'), may hold values from -12288 to 0, as said below
- gates_broad: float32 [12288, 8], P('sp', 'tp'), may hold values from -12288 to 0, as said below
- project_narrow: bfloat16 [512, 2048], P('tp'), may hold values from -0.5 to 0.5
- project_broad: bfloat16 [512, 2048], P('tp'), may hold values from -0.5 to 0.5
- norm_gain: float32 [2048], replicated, may hold values from 0.1 to 1.9
- up_weight: bfloat16 [2048, 8192], P('sp', 'tp'), may hold values from -0.125 to 0.125
- down_weight: bfloat16 [8192, 2048], P('tp', 'sp'), may hold values from -0.0625 to 0.0625
Outputs:
- layer_out: bfloat16 [12288, 2048], P(('sp', 'tp'))
Inputs may be any that keep to these rules, and one draw needn't show every extreme that they name: `gates_narrow`: each head's cumulative log gate never rises from one position to the next. `gates_broad`: each head's cumulative log gate never rises from one position to the next.
All inputs are finite; a program needn't handle non-finite values.
Results may differ from a plain program's by a relative error of at most 0.018.
Values may be sent and summed in bfloat16 or wider, within the bound.
A program may use at most 128 MiB of HBM per device.

v0:
```python
import jax
import jax.numpy as jnp
from jax import lax
from jax.sharding import PartitionSpec as P

A_DIM = 32
B_DIM = 64


def gather_turned(arrays, axis, dims):
    turned = [jnp.moveaxis(a, dim, 0) for a, dim in zip(arrays, dims)]
    widths = [t[0].size for t in turned]
    both = jnp.concatenate([t.reshape(-1, w) for t, w in zip(turned, widths)], axis=1)
    whole = lax.all_gather(both, axis, axis=0, tiled=True)
    tiles = jnp.split(whole, [sum(widths[:k]) for k in range(1, len(widths))], axis=1)
    return tuple(
        (
            jnp.moveaxis(b.reshape(-1, *t.shape[1:]), 0, dim)
            for b, t, dim in zip(tiles, turned, dims)
        )
    )


def in_one_piece(arrays, axis, dim, along):
    widths = [a.shape[along] for a in arrays]
    both = jnp.concatenate(arrays, axis=along)
    whole = lax.all_gather(both, axis, axis=dim, tiled=True)
    return tuple(jnp.split(whole, [sum(widths[:k]) for k in range(1, len(widths))], axis=along))


def cut_along(value, dim, size):
    before, after = (value.shape[:dim], value.shape[dim + 1 :])
    return jnp.moveaxis(value.reshape(*before, size, -1, *after), dim, 0)


def sent_and_summed(value, axis, dim):
    tiles = cut_along(value, dim, lax.axis_size(axis))
    arrived = lax.all_to_all(tiles, axis, split_axis=0, concat_axis=0, tiled=True)
    return arrived.astype(jnp.float32).sum(axis=0)


def laid_out(tiles, dim):
    tiles = jnp.moveaxis(tiles, 0, dim)
    shape = tiles.shape
    return tiles.reshape(*shape[:dim], shape[dim] * shape[dim + 1], *shape[dim + 2 :])


def copy_for_each(value, axis):
    size = lax.axis_size(axis)
    return lax.all_to_all(
        jnp.broadcast_to(value[None], (size, *value.shape)), axis, 0, 0, tiled=True
    )


def gather_directly(value, axis, dim):
    return laid_out(copy_for_each(value, axis), dim)


def group_update(state, queries, keys, values, query_gates, key_gates, allowed, head_size):
    peak, total, summed = state
    query_count = queries.shape[0]
    key_count = keys.shape[0]
    heads = queries.shape[1] // head_size
    scores = jnp.einsum(
        "qhd,khd->hqk",
        queries.reshape(query_count, heads, head_size),
        keys.reshape(key_count, heads, head_size),
        preferred_element_type=jnp.float32,
    ) * head_size ** (-0.5)
    scores = scores + query_gates.T[:, :, None] - key_gates.T[:, None, :]
    scores = jnp.where(allowed[None], scores, -1e30)
    new_peak = jnp.maximum(peak, jnp.max(scores, axis=-1))
    weights = jnp.exp(scores - new_peak[..., None]) * allowed[None].astype(jnp.float32)
    total = jnp.sum(weights, axis=-1)
    summed = jnp.einsum(
        "hqk,khd->hqd",
        weights.astype(jnp.bfloat16),
        values.reshape(key_count, heads, head_size),
        preferred_element_type=jnp.float32,
    )
    return (new_peak, total, summed)


def empty_state(query_count, heads, head_size):
    return (
        jnp.full((heads, query_count), -1e30, jnp.float32),
        jnp.zeros((heads, query_count), jnp.float32),
        jnp.zeros((heads, query_count, head_size), jnp.float32),
    )


def finish_group(state, head_size):
    peak, total, summed = state
    result = summed / total[..., None]
    return (
        result.transpose(1, 0, 2)
        .reshape(result.shape[1], result.shape[0] * head_size)
        .astype(jnp.bfloat16)
    )


def rms_scaled(mixed, norm_gain):
    mixed_wide = mixed.astype(jnp.float32)
    scale = lax.rsqrt(jnp.mean(mixed_wide * mixed_wide, axis=-1, keepdims=True) + 1e-06)
    return (mixed_wide * scale * norm_gain).astype(jnp.bfloat16)


def local(
    residual,
    queries_narrow,
    keys_narrow,
    values_narrow,
    queries_broad,
    keys_broad,
    values_broad,
    gates_narrow,
    gates_broad,
    project_narrow,
    project_broad,
    norm_gain,
    up_weight,
    down_weight,
):
    up_whole, down_whole = gather_turned((up_weight, down_weight), "sp", (0, 1))
    local_count = queries_narrow.shape[0]
    table_narrow, table_broad = in_one_piece((gates_narrow, gates_broad), "sp", 0, 1)
    query_pos = lax.axis_index("sp") * local_count + jnp.arange(local_count, dtype=jnp.int32)
    initial = (
        empty_state(local_count, queries_narrow.shape[1] // A_DIM, A_DIM),
        empty_state(local_count, queries_broad.shape[1] // B_DIM, B_DIM),
    )
    piece_keys_narrow, piece_values_narrow, piece_keys_broad, piece_values_broad = in_one_piece(
        (keys_narrow, values_narrow, keys_broad, values_broad), "sp", 0, 1
    )
    piece_count = piece_keys_narrow.shape[0]
    key_pos = jnp.arange(piece_count, dtype=jnp.int32)
    allowed = key_pos[None, :] <= query_pos[:, None]
    state_narrow = group_update(
        initial[0],
        queries_narrow,
        piece_keys_narrow,
        piece_values_narrow,
        gates_narrow,
        table_narrow,
        allowed,
        A_DIM,
    )
    state_broad = group_update(
        initial[1],
        queries_broad,
        piece_keys_broad,
        piece_values_broad,
        gates_broad,
        table_broad,
        allowed,
        B_DIM,
    )
    attended_narrow = finish_group(state_narrow, A_DIM)
    attended_broad = finish_group(state_broad, B_DIM)
    projected = sent_and_summed(
        (
            jnp.dot(attended_narrow, project_narrow, preferred_element_type=jnp.float32)
            + jnp.dot(attended_broad, project_broad, preferred_element_type=jnp.float32)
        ).astype(jnp.bfloat16),
        "tp",
        0,
    )
    mixed = (residual.astype(jnp.float32) + projected).astype(jnp.bfloat16)
    features = gather_directly(rms_scaled(mixed, norm_gain), "tp", 0)
    up_total = jnp.dot(features, up_whole, preferred_element_type=jnp.float32)
    hidden = jnp.square(jax.nn.relu(up_total)).astype(jnp.bfloat16)
    down_term = jnp.dot(hidden, down_whole, preferred_element_type=jnp.float32)
    summed_rows = sent_and_summed(down_term.astype(jnp.bfloat16), "tp", 0)
    return (mixed.astype(jnp.float32) + summed_rows).astype(jnp.bfloat16)


def solution(mesh):
    return jax.shard_map(
        local,
        mesh=mesh,
        in_specs=(
            P(("sp", "tp"), None),
            P("sp", "tp"),
            P("sp", "tp"),
            P("sp", "tp"),
            P("sp", "tp"),
            P("sp", "tp"),
            P("sp", "tp"),
            P("sp", "tp"),
            P("sp", "tp"),
            P("tp", None),
            P("tp", None),
            P(),
            P("sp", "tp"),
            P("tp", "sp"),
        ),
        out_specs=P(("sp", "tp"), None),
        check_vma=False,
    )
```

profile of v0, /device:TPU:1, one launch (start us, length us, event | category | flops | bytes accessed | tf_op | source)
XLA Modules:
  0.0 236.2 jit_solution(15525705607520377519)
XLA Ops:
  6.5 0.9 copy.16
  7.4 0.9 copy.17
  8.3 0.9 copy.18
  9.2 0.9 copy.19
  10.1 0.8 pad_maximum_fusion.1
  10.9 1.5 pad_maximum_fusion
  12.5 0.7 maximum_bitcast_fusion
  13.2 47.3 %all-gather = f32[64,192,3]{1,2,0:T(4,128)S(1)} all-gather(f32[1,192,3]{1,2,0:T(4,128)S(1)} %maximum_bitcast_fusion), channel_id=1, replica_groups=mesh['sp'=64,'tp'=8] {'sp'}, dimensions={0}, use_global_device_ids=true | all-gather | bytes 149760 | tf_op jit(solution)/shard_map/all_gather | solution.py:27
  61.3 6.1 %fusion.8 = (f32[192,12288]{1,0:T(8,128)}, pred[192,12288]{1,0:T(8,128)(4,1)}) fusion(s32[192]{0:T(256)S(1)} %iota_add_fusion), kind=kLoop, calls=%fused_computation.12 | loop fusion | flops 4718592 | bytes 11797248 | tf_op jit(solution)/shard_map/convert_element_type | solution.py:73
  67.4 38.5 %all-gather.4.cloned.1.call-done = bf16[12288,256]{1,0:T(8,128)(2,1)} async-done(((bf16[192,256]{1,0:T(8,128)(2,1)}), bf16[12288,256]{1,0:T(8,128)(2,1)}) %all-gather.4.cloned.1.call-update) | async-done | bytes 6291472 | tf_op jit(solution)/shard_map/all_gather | solution.py:27
  105.9 4.7 %fusion.66 = (bf16[12288,64]{1,0:T(8,128)(2,1)}, bf16[12288,64]{1,0:T(8,128)(2,1)S(1)}) fusion(bf16[12288,256]{1,0:T(8,128)(2,1)} %all-gather.4.cloned.1.call-done), kind=kLoop, calls=%fused_computation.55 | loop fusion | bytes 6291456 | tf_op jit(solution)/shard_map/split | solution.py:28
  110.6 4.3 %copy.20 = bf16[12288,64]{0,1:T(8,128)(2,1)} copy(bf16[12288,64]{1,0:T(8,128)(2,1)} %get-tuple-element.7) | data formatting | bytes 3145728 | tf_op jit(solution)/shard_map/split | solution.py:28
  114.9 2.4 %copy.22 = bf16[12288,64]{0,1:T(8,128)(2,1)} copy(bf16[12288,64]{1,0:T(8,128)(2,1)S(1)} %get-tuple-element.8) | data formatting | bytes 3145728 | tf_op jit(solution)/shard_map/split | solution.py:28
  117.3 8.4 %fusion.68 = (f32[192]{0:T(256)S(1)}, f32[192,12288]{1,0:T(8,128)}) fusion(f32[12288]{0:T(1024)S(1)} %bitcast.47, f32[192]{0:T(256)} %bitcast.50, bf16[192,64]{0,1:T(8,128)(2,1)} %param.18, bf16[12288,256]{1,0:T(8,128)(2,1)} %all-gather.4.cloned.1.call-done, s32[192]{0:T(256)} %copy-done.6), kind=kOutput, calls=%fused_computation.57 | convolution fusion | flops 316145472 | bytes 12667648 | tf_op jit(solution)/shard_map/qhd,khd->hqk/dot_general | solution.py:64
  125.8 9.7 %fusion.67 = (f32[2,192]{1,0:T(2,128)S(1)}, f32[2,192,12288]{2,1,0:T(8,128)}) fusion(f32[2,12288]{1,0:T(2,128)S(1)} %slice_bitcast_fusion, f32[2,192]{1,0:T(2,128)S(1)} %bitcast.49, bf16[12288,2,32]{0,2,1:T(8,128)(2,1)S(1)} %bitcast.41, bf16[192,2,32]{0,2,1:T(8,128)(2,1)S(1)} %bitcast.51, pred[192,12288]{1,0:T(8,128)(4,1)S(1)} %copy-done.2), kind=kOutput, calls=%fused_computation.56 | convolution fusion | flops 325582464 | bytes 22932480 | tf_op jit(solution)/shard_map/qhd,khd->hqk/dot_general | solution.py:64
  135.6 8.5 %fusion.3 = f32[2,192]{1,0:T(2,128)S(1)} fusion(f32[2,192,12288]{2,1,0:T(8,128)} %get-tuple-element.12, f32[192,12288]{1,0:T(8,128)S(1)} %bitcast.39, f32[2,192]{1,0:T(2,128)S(1)} %broadcast_maximum_fusion), kind=kLoop, calls=%fused_computation.6 | loop fusion | flops 14155392 | bytes 28314624 | tf_op jit(solution)/shard_map/reduce_sum | solution.py:74
  144.1 8.5 %fusion.40 = bf16[192,2,32]{0,2,1:T(8,128)(2,1)S(1)} fusion(bf16[12288,2,32]{0,2,1:T(8,128)(2,1)S(1)} %bitcast.40, f32[2,192,12288]{2,1,0:T(8,128)} %get-tuple-element.12, f32[192,12288]{1,0:T(8,128)S(1)} %bitcast.39, f32[2,192]{1,0:T(2,128)S(1)} %broadcast_maximum_fusion, f32[192,2]{0,1:T(2,128)S(1)} %bitcast.48), kind=kOutput, calls=%fused_computation.32 | convolution fusion | flops 316170240 | bytes 29912064 | tf_op jit(solution)/shard_map/hqk,khd->hqd/dot_general | solution.py:75
  153.0 6.1 %fusion.9 = f32[192]{0:T(256)S(1)} fusion(f32[192,12288]{1,0:T(8,128)} %get-tuple-element.14, f32[192]{0:T(256)S(1)} %broadcast_maximum_fusion.1, s32[192]{0:T(256)S(1)} %copy-done.7), kind=kLoop, calls=%fused_computation.13 | loop fusion | flops 9436992 | bytes 9439488 | tf_op jit(solution)/shard_map/reduce_sum | solution.py:74
  159.1 8.7 %fusion.22 = bf16[192,2048]{1,0:T(8,128)(2,1)S(1)} fusion(f32[192,2048]{1,0:T(8,128)S(1)} %fusion.69, bf16[64,2048]{1,0:T(8,128)(2,1)S(1)} %copy-done.9, bf16[12288,256]{1,0:T(8,128)(2,1)} %all-gather.4.cloned.1.call-done, f32[192,12288]{1,0:T(8,128)} %get-tuple-element.14, f32[192]{0:T(256)S(1)} %broadcast_maximum_fusion.1, s32[192]{0:T(256)S(1)} %copy-done.7, ...), kind=kOutput, calls=%fused_computation.24 | convolution fusion | flops 362569728 | bytes 15206656 | tf_op jit(solution)/shard_map/dot_general | solution.py:163
  167.8 18.1 %all_to_all.15 = bf16[8,24,2048]{2,1,0:T(8,128)(2,1)S(1)} all-to-all(bf16[8,24,2048]{2,1,0:T(8,128)(2,1)S(1)} %bitcast.42), channel_id=1, replica_groups=mesh['sp'=64,'tp'=8] {'tp'}, dimensions={0} | all-to-all | bytes 1572864 | tf_op jit(solution)/shard_map/all_to_all | solution.py:38
  186.4 15.6 %all_to_all.16 = bf16[8,24,2048]{2,1,0:T(8,128)(2,1)S(1)} all-to-all(bf16[8,24,2048]{2,1,0:T(8,128)(2,1)S(1)} %broadcast_in_dim.27), channel_id=1, replica_groups=mesh['sp'=64,'tp'=8] {'tp'}, dimensions={0} | all-to-all | bytes 1572864 | tf_op jit(solution)/shard_map/all_to_all | solution.py:50
  202.0 3.7 %all-gather.6.cloned.1.call-done = bf16[2048,2048]{1,0:T(8,128)(2,1)} async-done(((bf16[32,2048]{1,0:T(8,128)(2,1)}), bf16[2048,2048]{1,0:T(8,128)(2,1)}) %all-gather.6.cloned.1.call-update) | async-done | bytes 8388624 | tf_op jit(solution)/shard_map/all_gather | solution.py:14
  205.7 5.8 %fusion.19 = bf16[192,2048]{1,0:T(8,128)(2,1)S(1)} fusion(bf16[2048,2048]{1,0:T(8,128)(2,1)} %all-gather.6.cloned.1.call-done, bf16[192,2048]{1,0:T(8,128)(2,1)S(1)} %bitcast.43), kind=kOutput, calls=%fused_computation.23 | convolution fusion | flops 1611595776 | bytes 9961472 | tf_op jit(solution)/shard_map/dot_general | solution.py:172
  211.5 17.1 %all_to_all.17 = bf16[8,24,2048]{2,1,0:T(8,128)(2,1)S(1)} all-to-all(bf16[8,24,2048]{2,1,0:T(8,128)(2,1)S(1)} %bitcast.44), channel_id=1, replica_groups=mesh['sp'=64,'tp'=8] {'tp'}, dimensions={0} | all-to-all | bytes 1572864 | tf_op jit(solution)/shard_map/all_to_all | solution.py:38
  (48 shorter events, 2.5 us)
Async XLA Ops:
  6.5 146.0 %copy-start = (bf16[64,2048]{1,0:T(8,128)(2,1)S(1)}, bf16[64,2048]{1,0:T(8,128)(2,1)}, u32[]{:S(2)}) copy-start(bf16[64,2048]{1,0:T(8,128)(2,1)} %param.23) | copy-start | bytes 786436
  6.5 99.4 %all-gather.4.cloned.1.call-start = ((), (), s32[]{:S(2)}) async-start(), calls=%async_computation.3 | async-start | bytes 6389760 | tf_op jit(solution)/shard_map/all_gather | solution.py:27
  10.9 194.8 %all-gather.6.cloned.1.call-start = ((), (), s32[]{:S(2)}) async-start(), calls=%async_computation.4 | async-start | bytes 8519680 | tf_op jit(solution)/shard_map/all_gather | solution.py:14
  60.8 0.5 copy-start.6
  117.3 8.5 %copy-start.2 = (pred[192,12288]{1,0:T(8,128)(4,1)S(1)}, pred[192,12288]{1,0:T(8,128)(4,1)}, u32[]{:S(2)}) copy-start(pred[192,12288]{1,0:T(8,128)(4,1)} %get-tuple-element.10) | copy-start | bytes 7077892
  117.3 8.5 %copy-start.3 = (bf16[12288,64]{0,1:T(8,128)(2,1)S(1)}, bf16[12288,64]{0,1:T(8,128)(2,1)}, u32[]{:S(2)}) copy-start(bf16[12288,64]{0,1:T(8,128)(2,1)} %copy.20) | copy-start | bytes 4718596
  117.3 8.5 %copy-start.8 = (f32[192,2]{0,1:T(2,128)S(1)}, f32[192,2]{0,1:T(2,128)}, u32[]{:S(2)}) copy-start(f32[192,2]{0,1:T(2,128)} %param.21) | copy-start | bytes 4612
  117.3 8.5 %copy-start.10 = (bf16[192,64]{0,1:T(8,128)(2,1)S(1)}, bf16[192,64]{0,1:T(8,128)(2,1)}, u32[]{:S(2)}) copy-start(bf16[192,64]{0,1:T(8,128)(2,1)} %param.15) | copy-start | bytes 73732
  117.3 18.2 %slice-start = ((s8[9437184]{0:T(1024)(128)(4,1)}), s8[4194304]{0:T(1024)(128)(4,1)S(1)}, s32[]{:S(2)}) async-start(s8[9437184]{0:T(1024)(128)(4,1)} %bitcast.38), calls=%async_computation.5 | async-start | bytes 8388608
  117.3 18.2 %slice-start.1 = ((s8[9437184]{0:T(1024)(128)(4,1)}), s8[4194304]{0:T(1024)(128)(4,1)S(1)}, s32[]{:S(2)}) async-start(s8[9437184]{0:T(1024)(128)(4,1)} %bitcast.38), calls=%async_computation.6 | async-start | bytes 8388608
  125.8 9.7 %slice-start.2 = ((s8[9437184]{0:T(1024)(128)(4,1)}), s8[1048576]{0:T(1024)(128)(4,1)S(1)}, s32[]{:S(2)}) async-start(s8[9437184]{0:T(1024)(128)(4,1)} %bitcast.38), calls=%async_computation.7 | async-start | bytes 2097152
  135.5 8.5 %copy-start.1 = (bf16[12288,64]{0,1:T(8,128)(2,1)S(1)}, bf16[12288,64]{0,1:T(8,128)(2,1)}, u32[]{:S(2)}) copy-start(bf16[12288,64]{0,1:T(8,128)(2,1)} %copy.22) | copy-start | bytes 4718596
  144.1 8.9 %copy-start.7 = (s32[192]{0:T(256)S(1)}, s32[192]{0:T(256)}, u32[]{:S(2)}) copy-start(s32[192]{0:T(256)} %copy-done.6) | copy-start | bytes 2308
  152.6 6.5 %copy-start.9 = (bf16[64,2048]{1,0:T(8,128)(2,1)S(1)}, bf16[64,2048]{1,0:T(8,128)(2,1)}, u32[]{:S(2)}) copy-start(bf16[64,2048]{1,0:T(8,128)(2,1)} %param.24) | copy-start | bytes 786436
  159.1 26.9 %copy-start.4 = (bf16[24,2048]{1,0:T(8,128)(2,1)S(1)}, bf16[24,2048]{1,0:T(8,128)(2,1)}, u32[]{:S(2)}) copy-start(bf16[24,2048]{1,0:T(8,128)(2,1)} %param.14) | copy-start | bytes 294916
  159.1 27.1 %copy-start.5 = (f32[2048]{0:T(1024)S(1)}, f32[2048]{0:T(1024)}, u32[]{:S(2)}) copy-start(f32[2048]{0:T(1024)} %param.25) | copy-start | bytes 24580
Sparse Core Ops, SparseCore 0:
  11.0 94.8 all-gather.3
  109.0 96.6 all-gather.5
where the time goes:
time: 237 us; the launch traced here: 236 us
  blocking collectives  98 us (41%)
  waiting for transfers between devices  42.2 us (18%)
  matrix products  41.5 us (18%)
  other arithmetic  24.9 us (11%)
  local copies, waits for them, and re-layouts  15.8 us (7%)
  between operations  13.6 us (6%)
    all_gather x1, blocking collectives, in_one_piece(): whole = lax.all_gather(both, axis, axis=dim, tiled=True)  47.3 us
    all_gather x1, waiting for transfers between devices, in_one_piece(): whole = lax.all_gather(both, axis, axis=dim, tiled=True)  38.5 us
    all_to_all x2, blocking collectives, sent_and_summed(): lax.all_to_all(tiles, axis, split_axis=0, concat_axis=0, tiled=True)  35.2 us
    dot_general x2, matrix products, group_update(): jnp.einsum('qhd,khd->hqk', queries.reshape(query_count, heads, head_size)...  18.2 us
    all_to_all x1, blocking collectives, copy_for_each(): lax.all_to_all(jnp.broadcast_to(value[None], (size, *value.shape)), axis,...  15.6 us
    reduce_sum x2, other arithmetic, group_update(): total = jnp.sum(weights, axis=-1)  14.6 us
    split x4, local copies, waits for them, and re-layouts, in_one_piece(): jnp.split(whole, [sum(widths[:k]) for k in range(1, len(widths))], axis=a...  11.4 us
    dot_general x1, matrix products, local(): jnp.dot(attended_broad, project_broad, preferred_element_type=jnp.float32)  8.71 us
  transfers between devices with their start and end apart: 2, of which 2 were waited for; matrix products, arithmetic and copies ran while one was open for 30% of the time, Pallas kernels for 0%

commit v1 on v0

v1 whole, which is shorter than its diff:
```python
import functools

import jax
import jax.numpy as jnp
from jax import lax
from jax.experimental import pallas as pl
from jax.experimental.pallas import tpu as pltpu
from jax.sharding import PartitionSpec as P

A_DIM = 32
B_DIM = 64
LOG2E = 1.4426950408889634
FAR = 1e30
MESH = pl.DeviceIdType.MESH
BF = jnp.bfloat16
F32 = jnp.float32


def split_sp(mesh):
    size = mesh.shape["sp"]
    ny = 1
    while ny * ny < size:
        ny *= 2
    return size // ny, ny


def rcopy(src, dst, send, recv, device):
    return pltpu.make_async_remote_copy(
        src_ref=src,
        dst_ref=dst,
        send_sem=send,
        recv_sem=recv,
        device_id=device,
        device_id_type=MESH,
    )


def nt_dot(a, b):
    return lax.dot_general(a, b, (((1,), (1,)), ((), ())), preferred_element_type=F32)


def head_mask(shape):
    lane = lax.broadcasted_iota(jnp.int32, shape, 1)
    return (lane < A_DIM, (lane >= A_DIM) & (lane < 2 * A_DIM), lane >= 2 * A_DIM)


SCALES = (A_DIM**-0.5 * LOG2E, A_DIM**-0.5 * LOG2E, B_DIM**-0.5 * LOG2E)


class Tp:
    def __init__(self, nx, buf, xs, xr, ds, dr):
        self.nx, self.buf, self.xs, self.xr, self.ds, self.dr = nx, buf, xs, xr, ds, dr
        self.sp, self.tp = lax.axis_index("sp"), lax.axis_index("tp")
        self.x, self.c = self.tp // 2, self.tp % 2

    def across(self, i):
        to = ((self.x + i) % self.nx) * 2 + self.c
        return rcopy(
            self.buf.at[self.tp], self.buf.at[self.tp], self.xs.at[i - 1], self.xr.at[i - 1], (self.sp, to)
        )

    def arrived(self, i):
        return ((self.x - i + self.nx) % self.nx) * 2 + self.c

    def beside(self, i):
        src = self.arrived(i)
        return rcopy(
            self.buf.at[src], self.buf.at[src], self.ds.at[i], self.dr.at[i], (self.sp, self.x * 2 + 1 - self.c)
        )

    def start(self):
        for i in range(1, self.nx):
            self.across(i).start()
        self.beside(0).start()

    def forward(self, i):
        self.across(i).wait_recv()
        self.beside(i).start()

    def finish(self):
        for i in range(self.nx):
            self.beside(i).wait_recv()
        for i in range(1, self.nx):
            self.across(i).wait_send()
        for i in range(self.nx):
            self.beside(i).wait_send()


def front(
    nz,
    ny,
    nt,
    qn,
    qb,
    kn,
    kb,
    vn,
    vb,
    gn,
    gb,
    pn,
    pb,
    res,
    gain,
    mixed_out,
    feat_out,
    qbuf,
    kbuf,
    vbuf,
    gbuf,
    gk,
    pw,
    osend,
    lsend,
    orecv,
    lrecv,
    asend,
    arecv,
    feat,
    pw_in,
    q_s,
    q_r,
    kv_s,
    kv_r,
    pw_xs,
    pw_xr,
    pw_ds,
    pw_dr,
    p_s,
    p_r,
    a_s,
    a_r,
    f_xs,
    f_xr,
    f_ds,
    f_dr,
):
    nx = nt // 2
    sp, tp = lax.axis_index("sp"), lax.axis_index("tp")
    z, y = sp // ny, sp % ny
    tok = qn.shape[0]
    rows = tok // nt
    keys = nz * tok
    d = res.shape[1]

    qbuf[y, 0:tok, 0:64] = qn[...]
    qbuf[y, 0:tok, 64:128] = qb[...]
    kbuf[0, :, 0:64] = kn[...]
    kbuf[0, :, 64:128] = kb[...]
    vbuf[0, :, 0:64] = vn[...]
    vbuf[0, :, 64:128] = vb[...]
    for r in range(nz):
        vbuf[r, :, 128:256] = jnp.ones((tok, 128), BF)
    lane = lax.broadcasted_iota(jnp.int32, (tok, 128), 1)
    gates = jnp.where(
        lane == 0,
        gn[:, 0:1],
        jnp.where(lane == 1, gn[:, 1:2], jnp.where(lane == 2, gb[:, 0:1], 0.0)),
    )
    qbuf[y, tok : tok + 16, :] = gates[0:16].astype(BF)
    gbuf[0, :, 0:tok] = jnp.transpose(gates)[0:8]
    gbuf[0, :, tok:256] = jnp.zeros((8, 256 - tok), F32)

    load_n = pltpu.make_async_copy(pn, pw.at[tp, 0:64], pw_in.at[0])
    load_b = pltpu.make_async_copy(pb, pw.at[tp, 64:128], pw_in.at[1])
    load_n.start()
    load_b.start()

    barrier = pltpu.get_barrier_semaphore()
    peers = [(z * ny + (y + i) % ny, tp) for i in range(1, ny)]
    up_z, down_z = ((z + 1) % nz) * ny + y, ((z + nz - 1) % nz) * ny + y
    peers += [(up_z, tp), (down_z, tp)]
    peers += [(sp, (tp + i) % nt) for i in range(1, nt)]
    for peer in peers:
        pl.semaphore_signal(barrier, inc=1, device_id=peer, device_id_type=MESH)
    pl.semaphore_wait(barrier, len(peers))

    def ring(slot, src, to):
        return [
            rcopy(kbuf.at[src], kbuf.at[slot], kv_s.at[0, slot - 1], kv_r.at[0, slot - 1], (to, tp)),
            rcopy(
                vbuf.at[src, :, 0:128],
                vbuf.at[slot, :, 0:128],
                kv_s.at[1, slot - 1],
                kv_r.at[1, slot - 1],
                (to, tp),
            ),
            rcopy(gbuf.at[src], gbuf.at[slot], kv_s.at[2, slot - 1], kv_r.at[2, slot - 1], (to, tp)),
        ]

    rights = nz // 2
    lefts = nz - 1 - rights
    steps = [ring(s, s - 1, up_z) for s in range(1, rights + 1)]
    steps_left = [ring(nz - s, (nz - s + 1) % nz, down_z) for s in range(1, lefts + 1)]

    q_sends = [
        rcopy(
            qbuf.at[y], qbuf.at[y], q_s.at[i - 1], q_r.at[i - 1], (z * ny + (y + i) % ny, tp)
        )
        for i in range(1, ny)
    ]
    for c in steps[0]:
        c.start()
    for chain in steps_left[0:1]:
        for c in chain:
            c.start()
    for c in q_sends:
        c.start()
    load_n.wait()
    load_b.wait()
    share = Tp(nx, pw, pw_xs, pw_xr, pw_ds, pw_dr)
    share.start()

    for s in range(1, rights + 1):
        for c in steps[s - 1]:
            c.wait_recv()
        if s < rights:
            for c in steps[s]:
                c.start()
        if s <= lefts:
            for c in steps_left[s - 1]:
                c.wait_recv()
            if s < lefts:
                for c in steps_left[s]:
                    c.start()

    for r in range(nz):
        gk[:, r * tok : (r + 1) * tok] = jnp.where(r <= z, gbuf[r, :, 0:tok], FAR)

    col = lax.broadcasted_iota(jnp.int32, (1, keys), 1)

    def block(src, own, out_o, out_l):
        q = qbuf[src, 0:tok, :]
        masks = head_mask((tok, 128))
        k = kbuf[...].reshape(keys, 128)
        v = vbuf[...].reshape(keys, 256)
        outs, lses = [], []
        for h in range(3):
            s = nt_dot(jnp.where(masks[h], q, jnp.zeros_like(q)), k)
            ref = qbuf[src, tok : tok + 16, :][0:1, h : h + 1].astype(F32)
            bias = (ref - gk[h : h + 1, :]) * LOG2E
            if not own:
                bias = jnp.where((col < tok) & (y > src), -FAR, bias)
            s = s * SCALES[h] + bias
            if own:
                wide = min(keys, 256)
                first = s[:, 0:wide]
                at = lax.broadcasted_iota(jnp.int32, first.shape, 1)
                row = lax.broadcasted_iota(jnp.int32, first.shape, 0)
                first = jnp.where((at < tok) & (at > row), -FAR, first)
                s = jnp.concatenate([first, s[:, wide:]], axis=1) if keys > wide else first
            m = jnp.max(s, axis=1, keepdims=True)
            w = jnp.exp2(s - m).astype(BF)
            o = jnp.dot(w, v, preferred_element_type=F32)
            total = o[:, 128:256]
            outs.append(o[:, 0:128] / total)
            lses.append(m + jnp.log2(total))
        out_o[...] = jnp.where(masks[0], outs[0], jnp.where(masks[1], outs[1], outs[2])).astype(BF)
        lse = jnp.where(lane == 0, lses[0], jnp.where(lane == 1, lses[1], lses[2]))
        out_l[:, 0:tok] = jnp.transpose(lse)[0:8]

    def give(i):
        src = (y + ny - i) % ny
        to = (z * ny + src, tp)
        return [
            rcopy(osend.at[i - 1], orecv.at[y], p_s.at[0, i - 1], p_r.at[0, i - 1], to),
            rcopy(lsend.at[i - 1], lrecv.at[y], p_s.at[1, i - 1], p_r.at[1, i - 1], to),
        ]

    def one(i, carry):
        src = (y + ny - i) % ny
        rcopy(qbuf.at[y], qbuf.at[src], q_s.at[i - 1], q_r.at[i - 1], (z * ny + src, tp)).wait_recv()
        block(src, False, osend.at[i - 1], lsend.at[i - 1])
        for c in give(i):
            c.start()
        return carry

    lax.fori_loop(1, ny, one, 0)
    block(y, True, orecv.at[y], lrecv.at[y])
    for i in range(1, nx):
        share.forward(i)
    for i in range(1, ny):
        for c in give(i):
            c.wait_recv()

    lse = [lrecv[j, :, 0:tok] for j in range(ny)]
    peak = functools.reduce(jnp.maximum, lse)
    parts = [jnp.exp2(a - peak) for a in lse]
    inv = 1.0 / functools.reduce(jnp.add, parts)
    share_t = jnp.transpose(jnp.concatenate([a * inv for a in parts], axis=0))
    masks = head_mask((tok, 128))
    att = jnp.zeros((tok, 128), F32)
    for j in range(ny):
        f = [share_t[:, 8 * j + h : 8 * j + h + 1] for h in range(3)]
        factor = jnp.where(masks[0], f[0], jnp.where(masks[1], f[1], f[2]))
        att = att + factor * orecv[j].astype(F32)
    for t in range(nt):
        asend[t] = att[t * rows : (t + 1) * rows].astype(BF)

    def hand(i):
        to = (tp + i) % nt
        return rcopy(asend.at[to], arecv.at[tp], a_s.at[i - 1], a_r.at[i - 1], (sp, to))

    for i in range(1, nt):
        hand(i).start()
    arecv[tp] = asend[tp]
    share.finish()
    for i in range(1, nt):
        hand(i).wait_recv()

    full = jnp.concatenate([arecv[t] for t in range(nt)], axis=1)
    projected = jnp.dot(full, pw[...].reshape(nt * 128, d), preferred_element_type=F32)
    mixed = (res[...].astype(F32) + projected).astype(BF)
    mixed_out[...] = mixed
    wide = mixed.astype(F32)
    scale = lax.rsqrt(jnp.mean(wide * wide, axis=-1, keepdims=True) + 1e-6)
    feat[tp] = (wide * scale * gain[...]).astype(BF)

    spread = Tp(nx, feat, f_xs, f_xr, f_ds, f_dr)
    spread.start()
    for i in range(1, nx):
        spread.forward(i)
    spread.finish()
    feat_out[...] = feat[...]

    for chain in steps + steps_left:
        for c in chain:
            c.wait_send()
    for c in q_sends:
        c.wait_send()
    for i in range(1, ny):
        for c in give(i):
            c.wait_send()
    for i in range(1, nt):
        hand(i).wait_send()


def ffn(nt, feat, mixed, w, out, up, down, part, pair, psum, got, w_in, pair_s, pair_r, g_s, g_r):
    nx = nt // 2
    sp, tp = lax.axis_index("sp"), lax.axis_index("tp")
    x, c = tp // 2, tp % 2
    rows, d = mixed.shape
    nsp, band = up.shape[0], up.shape[1]
    load_up = pltpu.make_async_copy(w.at[:, 0:band], up, w_in.at[0])
    load_down = pltpu.make_async_copy(w.at[:, band : 2 * band], down, w_in.at[1])
    load_up.start()
    load_down.start()

    barrier = pltpu.get_barrier_semaphore()
    beside = (sp, x * 2 + 1 - c)
    peers = [beside] + [(sp, ((x + i) % nx) * 2 + c) for i in range(1, nx)]
    for peer in peers:
        pl.semaphore_signal(barrier, inc=1, device_id=peer, device_id_type=MESH)
    pl.semaphore_wait(barrier, len(peers))

    load_up.wait()
    f = feat[...].reshape(nt * rows, d)
    ff = up.shape[2]
    h = jnp.dot(f, up[...].reshape(nsp * band, ff), preferred_element_type=F32)
    h = jnp.square(jnp.maximum(h, 0.0)).astype(BF)
    load_down.wait()
    total = nt_dot(h, down[...].reshape(nsp * band, ff))
    for t in range(nt):
        block = total[t * rows : (t + 1) * rows]

        @pl.when(c == t % 2)
        def _():
            part[t // 2] = block

        @pl.when(c != t % 2)
        def _():
            psum[t // 2] = block.astype(BF)

    swap = rcopy(psum, pair, pair_s, pair_r, beside)
    swap.start()
    swap.wait()

    def give(i):
        to = (x + i) % nx
        return rcopy(psum.at[to], got.at[i - 1], g_s.at[i - 1], g_r.at[i - 1], (sp, to * 2 + c))

    for i in range(1, nx):
        to = (x + i) % nx
        psum[to] = (part[to] + pair[to].astype(F32)).astype(BF)
        give(i).start()
    acc = mixed[...].astype(F32) + (part[x] + pair[x].astype(F32))
    for i in range(1, nx):
        give(i).wait_recv()
        acc = acc + got[i - 1].astype(F32)
    out[...] = acc.astype(BF)
    for i in range(1, nx):
        give(i).wait_send()


def local(nz, ny, nt, *args):
    res, qn, kn, vn, qb, kb, vb, gn, gb, pn, pb, gain, up, down = args
    tok = qn.shape[0]
    rows, d = res.shape
    nx = nt // 2
    band, ff = up.shape
    nsp = nz * ny
    w = jnp.concatenate([up, down.T], axis=0)
    w = lax.all_gather(w, "sp", axis=0, tiled=True).reshape(nsp, 2 * band, ff)

    dma = pltpu.SemaphoreType.DMA
    vmem = pl.BlockSpec(memory_space=pltpu.VMEM)
    anyw = pl.BlockSpec(memory_space=pl.ANY)
    mixed, feat = pl.pallas_call(
        functools.partial(front, nz, ny, nt),
        out_shape=(
            jax.ShapeDtypeStruct((rows, d), BF),
            jax.ShapeDtypeStruct((nt, rows, d), BF),
        ),
        in_specs=[vmem] * 8 + [anyw] * 2 + [vmem] * 2,
        out_specs=(vmem, vmem),
        scratch_shapes=[
            pltpu.VMEM((ny, tok + 16, 128), BF),
            pltpu.VMEM((nz, tok, 128), BF),
            pltpu.VMEM((nz, tok, 256), BF),
            pltpu.VMEM((nz, 8, 256), F32),
            pltpu.VMEM((8, nz * tok), F32),
            pltpu.VMEM((nt, 128, d), BF),
            pltpu.VMEM((ny - 1, tok, 128), BF),
            pltpu.VMEM((ny - 1, 8, 256), F32),
            pltpu.VMEM((ny, tok, 128), BF),
            pltpu.VMEM((ny, 8, 256), F32),
            pltpu.VMEM((nt, rows, 128), BF),
            pltpu.VMEM((nt, rows, 128), BF),
            pltpu.VMEM((nt, rows, d), BF),
            dma((2,)),
            dma((ny - 1,)),
            dma((ny - 1,)),
            dma((3, nz - 1)),
            dma((3, nz - 1)),
            dma((nx - 1,)),
            dma((nx - 1,)),
            dma((nx,)),
            dma((nx,)),
            dma((2, ny - 1)),
            dma((2, ny - 1)),
            dma((nt - 1,)),
            dma((nt - 1,)),
            dma((nx - 1,)),
            dma((nx - 1,)),
            dma((nx,)),
            dma((nx,)),
        ],
        compiler_params=pltpu.CompilerParams(
            collective_id=0, has_side_effects=True, vmem_limit_bytes=48 * 1024 * 1024
        ),
        cost_estimate=pl.CostEstimate(
            flops=8_000_000_000, bytes_accessed=60_000_000, transcendentals=7_000_000
        ),
        name="front",
    )(qn, qb, kn, kb, vn, vb, gn, gb, pn, pb, res, gain.reshape(1, d))

    return pl.pallas_call(
        functools.partial(ffn, nt),
        out_shape=jax.ShapeDtypeStruct((rows, d), BF),
        in_specs=[vmem, vmem, anyw],
        out_specs=vmem,
        scratch_shapes=[
            pltpu.VMEM((nsp, band, ff), BF),
            pltpu.VMEM((nsp, band, ff), BF),
            pltpu.VMEM((nx, rows, d), F32),
            pltpu.VMEM((nx, rows, d), BF),
            pltpu.VMEM((nx, rows, d), BF),
            pltpu.VMEM((nx - 1, rows, d), BF),
            dma((2,)),
            dma,
            dma,
            dma((nx - 1,)),
            dma((nx - 1,)),
        ],
        compiler_params=pltpu.CompilerParams(
            collective_id=1, has_side_effects=True, vmem_limit_bytes=48 * 1024 * 1024
        ),
        cost_estimate=pl.CostEstimate(
            flops=1_600_000_000, bytes_accessed=20_000_000, transcendentals=0
        ),
        name="ffn",
    )(feat, mixed, w)


def solution(mesh):
    nz, ny = split_sp(mesh)
    sp_tp = P("sp", "tp")
    return jax.shard_map(
        functools.partial(local, nz, ny, mesh.shape["tp"]),
        mesh=mesh,
        in_specs=(P(("sp", "tp"), None),)
        + (sp_tp,) * 8
        + (P("tp", None), P("tp", None), P(), sp_tp, P("tp", "sp")),
        out_specs=P(("sp", "tp"), None),
        check_vma=False,
    )
```

time: 237 us -> 141 us (0.59)
  blocking collectives: 98 us -> 0 us
  Pallas kernels: 0 us -> 80.8 us
  matrix products: 41.5 us -> 0 us
  other arithmetic: 24.9 us -> 1.52 us
  waiting for transfers between devices: 42.2 us -> 34 us
  local copies, waits for them, and re-layouts: 15.8 us -> 11 us
    pallas_call x0 -> x2, Pallas kernels: none -> 80.8 us  [the longest x1 64.9 us: local(): pl.pallas_call(functools.partial(front, nz, ny, nt), out_shape=(jax.Shape...]
    all_to_all x3 -> x0, blocking collectives: 50.8 us -> none  [the longest x2 35.2 us: sent_and_summed(): lax.all_to_all(tiles, axis, split_axis=0, concat_axis=0, tiled=True)]
    all_gather x1 -> x0, blocking collectives: 47.3 us -> none  [in_one_piece(): whole = lax.all_gather(both, axis, axis=dim, tiled=True)]
    dot_general x6 -> x0, matrix products: 41.5 us -> none  [the longest x2 18.2 us: group_update(): jnp.einsum('qhd,khd->hqk', queries.reshape(query_count, heads, head_size)...]
    reduce_sum x5 -> x0, other arithmetic: 15 us -> none  [the longest x2 14.6 us: group_update(): total = jnp.sum(weights, axis=-1)]
    split x4 -> x0, local copies, waits for them, and re-layouts: 11.4 us -> none  [in_one_piece(): jnp.split(whole, [sum(widths[:k]) for k in range(1, len(widths))], axis=a...]
    all_gather x2 -> x1, waiting for transfers between devices: 42.2 us -> 34 us  [local(): w = lax.all_gather(w, 'sp', axis=0, tiled=True).reshape(nsp, 2 * band, ff)]
    convert_element_type x3 -> x0, other arithmetic: 6.89 us -> none  [the longest x1 6.14 us: group_update(): allowed[None].astype(jnp.float32)]
  transfers between devices with their start and end apart: 2 -> 1, of which waited for: 2 -> 1; matrix products, arithmetic and copies ran while one was open for 30% -> 5% of each run, Pallas kernels for 0% -> 46%
where the time goes in v1:
time: 141 us
  Pallas kernels  80.8 us (57%)
  waiting for transfers between devices  34 us (24%)
  between operations  13.4 us (10%)
  local copies, waits for them, and re-layouts  11 us (8%)
  other arithmetic  1.52 us (1%)
    pallas_call x1, Pallas kernels, local(): pl.pallas_call(functools.partial(front, nz, ny, nt), out_shape=(jax.Shape...  64.9 us
    all_gather x1, waiting for transfers between devices, local(): w = lax.all_gather(w, 'sp', axis=0, tiled=True).reshape(nsp, 2 * band, ff)  34 us
    pallas_call x1, Pallas kernels, local(): pl.pallas_call(functools.partial(ffn, nt), out_shape=jax.ShapeDtypeStruct...  15.9 us
    unnamed x17, local copies, waits for them, and re-layouts  11 us
  transfers between devices with their start and end apart: 1, of which 1 were waited for; matrix products, arithmetic and copies ran while one was open for 5% of the time, Pallas kernels for 46%

profile of v1, /device:TPU:1, one launch (start us, length us, event | category | flops | bytes accessed | tf_op | source)
XLA Modules:
  0.0 140.7 jit_solution(15376266032119338480)
XLA Ops:
  6.5 0.0 all-gather.2.cloned.1.call-start
  6.5 1.5 %pad_maximum_fusion = bf16[64,1024]{1,0:T(8,128)(2,1)} fusion(bf16[32,1024]{1,0:T(8,128)(2,1)} %bitcast.5, bf16[32,1024]{1,0:T(8,128)(2,1)} %param.26), kind=kLoop, calls=%fused_computation | loop fusion | flops 262144 | bytes 262144 | tf_op jit(solution)/shard_map/concatenate | solution.py:402
  8.1 0.0 all-gather.2.cloned.1.call-update
  8.1 0.8 copy.21.gn
  8.9 0.8 copy.22.gb
  9.7 0.9 copy.15.qn
  10.6 0.9 copy.16.qb
  11.4 0.9 copy.17.kn
  12.3 0.9 copy.18.kb
  13.2 0.9 copy.19.vn
  14.1 0.9 copy.20.vb
  14.9 0.0 copy-start
  14.9 0.9 copy-done
  15.9 0.0 copy-start.1
  15.9 0.9 copy-done.1
  16.9 0.0 copy-start.2
  16.9 0.9 copy-done.2
  17.7 0.0 copy-start.3
  17.7 0.7 copy-done.3
  18.4 64.9 %front.1 = (bf16[24,2048]{1,0:T(8,128)(2,1)S(1)}, bf16[8,24,2048]{2,1,0:T(8,128)(2,1)S(1)}) custom-call(bf16[192,64]{1,0:T(8,128)(2,1)S(1)} %copy.15.qn, bf16[192,64]{1,0:T(8,128)(2,1)S(1)} %copy.16.qb, bf16[192,64]{1,0:T(8,128)(2,1)S(1)} %copy.17.kn, bf16[192,64]{1,0:T(8,128)(2,1)S(1)} %copy.18.kb, bf16[192,64]{1,0:T(8,128)(2,1)S(1)} %copy.19.vn, ...), custom_call_target="tpu_custom_call" | custom-call | flops 8000000000 | bytes 60000000 | tf_op jit(solution)/shard_map/front/pallas_call | solution.py:408
  83.3 34.0 %all-gather.2.cloned.1.call-done = bf16[4096,1024]{1,0:T(8,128)(2,1)} async-done(((bf16[64,1024]{1,0:T(8,128)(2,1)}), bf16[4096,1024]{1,0:T(8,128)(2,1)}) %all-gather.2.cloned.1.call-update) | async-done | bytes 8388624 | tf_op jit(solution)/shard_map/all_gather | solution.py:403
  117.3 15.9 %ffn.1 = bf16[24,2048]{1,0:T(8,128)(2,1)S(1)} custom-call(bf16[8,24,2048]{2,1,0:T(8,128)(2,1)S(1)} %get-tuple-element.7.feat, bf16[24,2048]{1,0:T(8,128)(2,1)S(1)} %get-tuple-element.8.mixed, bf16[64,64,1024]{2,1,0:T(8,128)(2,1)} %bitcast.4), custom_call_target="tpu_custom_call" | custom-call | flops 1600000000 | bytes 20000000 | tf_op jit(solution)/shard_map/ffn/pallas_call | solution.py:457
  133.2 0.6 copy.24
Async XLA Ops:
  6.5 110.7 %all-gather.2.cloned.1.call-start = ((), (), s32[]{:S(2)}) async-start(), calls=%async_computation | async-start | bytes 8519680 | tf_op jit(solution)/shard_map/all_gather | solution.py:403
  14.9 1.0 copy-start
  15.9 0.9 copy-start.1
  16.9 0.9 copy-start.2
  17.7 0.7 copy-start.3
Sparse Core Ops, SparseCore 0:
  10.4 106.8 all-gather.1

commit v2 on v1

--- a/solution.py
+++ b/solution.py
@@ -86,7 +86,97 @@
             self.beside(i).wait_send()
 
 
-def front(
+class Weights:
+    def __init__(self, nz, ny, up, down, s1, r1, s2, r2):
+        self.nz, self.ny = nz, ny
+        self.bufs = (up, down)
+        self.s1, self.r1, self.s2, self.r2 = s1, r1, s2, r2
+        self.sp, self.tp = lax.axis_index("sp"), lax.axis_index("tp")
+        self.z, self.y = self.sp // ny, self.sp % ny
+
+    def shifted(self, along_y, by):
+        if along_y:
+            return self.z, (self.y + by + self.ny) % self.ny
+        return (self.z + by + self.nz) % self.nz, self.y
+
+    def length(self, along_y):
+        return self.ny if along_y else self.nz
+
+    def copy(self, phase, half, way, s, chunk, by):
+        along_y = (half == 0) == (phase == 1)
+        sign = 1 - 2 * way
+        z, y = self.shifted(along_y, by)
+        buf = self.bufs[half]
+        if phase == 1:
+            ref = buf.at[z, y]
+            if s == self.length(along_y) // 2:
+                rows = buf.shape[2] // 2
+                ref = buf.at[z, y, way * rows : (way + 1) * rows]
+            send, recv = self.s1.at[half, way, s - 1], self.r1.at[half, way, s - 1]
+        else:
+            if along_y:
+                part = self.nz // 2
+                ref = buf.at[chunk * part : (chunk + 1) * part, y]
+            else:
+                part = self.ny // 2
+                ref = buf.at[z, chunk * part : (chunk + 1) * part]
+            send, recv = self.s2.at[half, way, s - 1, chunk], self.r2.at[half, way, s - 1, chunk]
+        tz, ty = self.shifted(along_y, sign)
+        return rcopy(ref, ref, send, recv, (tz * self.ny + ty, self.tp))
+
+    def sent(self, phase, half, way, s, chunk=0):
+        return self.copy(phase, half, way, s, chunk, -(1 - 2 * way) * (s - 1))
+
+    def landed(self, phase, half, way, s, chunk=0):
+        return self.copy(phase, half, way, s, chunk, -(1 - 2 * way) * s)
+
+    def last(self, phase, half):
+        return self.length((half == 0) == (phase == 1)) // 2
+
+    def streams(self):
+        return [(half, way) for half in (0, 1) for way in (0, 1)]
+
+    def chunks(self, half, way, s):
+        return (way,) if s == self.last(2, half) else (0, 1)
+
+    def start(self):
+        for half, way in self.streams():
+            self.sent(1, half, way, 1).start()
+
+    def step(self, s):
+        for half, way in self.streams():
+            if s <= self.last(1, half):
+                self.landed(1, half, way, s).wait_recv()
+                if s < self.last(1, half):
+                    self.sent(1, half, way, s + 1).start()
+
+    def lines(self):
+        for chunk in (0, 1):
+            for half, way in self.streams():
+                if chunk in self.chunks(half, way, 1):
+                    self.sent(2, half, way, 1, chunk).start()
+
+    def tick(self, k):
+        s, chunk = k // 2 + 1, k % 2
+        for half, way in self.streams():
+            if s <= self.last(2, half) and chunk in self.chunks(half, way, s):
+                self.landed(2, half, way, s, chunk).wait_recv()
+                if s < self.last(2, half) and chunk in self.chunks(half, way, s + 1):
+                    self.sent(2, half, way, s + 1, chunk).start()
+
+    def ticks(self):
+        return 2 * max(self.last(2, 0), self.last(2, 1))
+
+    def finish(self):
+        for half, way in self.streams():
+            for s in range(1, self.last(1, half) + 1):
+                self.sent(1, half, way, s).wait_send()
+            for s in range(1, self.last(2, half) + 1):
+                for chunk in self.chunks(half, way, s):
+                    self.sent(2, half, way, s, chunk).wait_send()
+
+
+def layer(
     nz,
     ny,
     nt,
@@ -100,10 +190,18 @@
     gb,
     pn,
     pb,
+    res_in,
+    gain_in,
+    up_in,
+    down_in,
+    out,
+    raw,
+    graw_n,
+    graw_b,
     res,
     gain,
-    mixed_out,
-    feat_out,
+    up,
+    down,
     qbuf,
     kbuf,
     vbuf,
@@ -117,7 +215,11 @@
     asend,
     arecv,
     feat,
-    pw_in,
+    part,
+    psum,
+    pair,
+    got,
+    in_sem,
     q_s,
     q_r,
     kv_s,
@@ -134,37 +236,22 @@
     f_xr,
     f_ds,
     f_dr,
+    w_s1,
+    w_r1,
+    w_s2,
+    w_r2,
+    pair_s,
+    pair_r,
+    g_s,
+    g_r,
 ):
     nx = nt // 2
     sp, tp = lax.axis_index("sp"), lax.axis_index("tp")
     z, y = sp // ny, sp % ny
-    tok = qn.shape[0]
-    rows = tok // nt
+    x, core = tp // 2, tp % 2
+    tok = qn.shape[1]
+    rows, d = res.shape
     keys = nz * tok
-    d = res.shape[1]
-
-    qbuf[y, 0:tok, 0:64] = qn[...]
-    qbuf[y, 0:tok, 64:128] = qb[...]
-    kbuf[0, :, 0:64] = kn[...]
-    kbuf[0, :, 64:128] = kb[...]
-    vbuf[0, :, 0:64] = vn[...]
-    vbuf[0, :, 64:128] = vb[...]
-    for r in range(nz):
-        vbuf[r, :, 128:256] = jnp.ones((tok, 128), BF)
-    lane = lax.broadcasted_iota(jnp.int32, (tok, 128), 1)
-    gates = jnp.where(
-        lane == 0,
-        gn[:, 0:1],
-        jnp.where(lane == 1, gn[:, 1:2], jnp.where(lane == 2, gb[:, 0:1], 0.0)),
-    )
-    qbuf[y, tok : tok + 16, :] = gates[0:16].astype(BF)
-    gbuf[0, :, 0:tok] = jnp.transpose(gates)[0:8]
-    gbuf[0, :, tok:256] = jnp.zeros((8, 256 - tok), F32)
-
-    load_n = pltpu.make_async_copy(pn, pw.at[tp, 0:64], pw_in.at[0])
-    load_b = pltpu.make_async_copy(pb, pw.at[tp, 64:128], pw_in.at[1])
-    load_n.start()
-    load_b.start()
 
     barrier = pltpu.get_barrier_semaphore()
     peers = [(z * ny + (y + i) % ny, tp) for i in range(1, ny)]
@@ -173,7 +260,43 @@
     peers += [(sp, (tp + i) % nt) for i in range(1, nt)]
     for peer in peers:
         pl.semaphore_signal(barrier, inc=1, device_id=peer, device_id_type=MESH)
+
+    def load(i, src, dst):
+        return pltpu.make_async_copy(src, dst, in_sem.at[i])
+
+    loads = [load(i, r, raw.at[i]) for i, r in enumerate((qn, qb, kn, kb, vn, vb))]
+    loads += [load(6, gn, graw_n), load(7, gb, graw_b)]
+    load_w = [load(8, up_in, up.at[z, y]), load(9, down_in, down.at[z, y])]
+    load_p = [load(10, pn, pw.at[tp, 0:64]), load(11, pb, pw.at[tp, 64:128])]
+    load_r = [load(12, res_in, res), load(13, gain_in, gain)]
+    for c in loads + load_w + load_p + load_r:
+        c.start()
+
+    for r in range(nz):
+        vbuf[r, :, 128:256] = jnp.ones((tok, 128), BF)
+    for c in loads:
+        c.wait()
+
+    qbuf[y, 0:tok, :] = jnp.transpose(raw[0:2].reshape(128, tok))
+    kbuf[0] = jnp.transpose(raw[2:4].reshape(128, tok))
+    vbuf[0, :, 0:128] = jnp.transpose(raw[4:6].reshape(128, tok))
+    lane = lax.broadcasted_iota(jnp.int32, (tok, 128), 1)
+    first_lane = lax.broadcasted_iota(jnp.int32, (16, 128), 1)
+    starts = jnp.where(
+        first_lane == 0,
+        graw_n[0:1, 0:1],
+        jnp.where(first_lane == 1, graw_n[1:2, 0:1], jnp.where(first_lane == 2, graw_b[0:1, 0:1], 0.0)),
+    )
+    qbuf[y, tok : tok + 16, :] = starts.astype(BF)
+    gbuf[0] = jnp.zeros((8, 256), F32)
+    gbuf[0, 0:2, 0:tok] = graw_n[...]
+    gbuf[0, 2:3, 0:tok] = graw_b[...]
+
+    for c in load_w + load_p:
+        c.wait()
     pl.semaphore_wait(barrier, len(peers))
+
+    weights = Weights(nz, ny, up, down, w_s1, w_r1, w_s2, w_r2)
 
     def ring(slot, src, to):
         return [
@@ -199,30 +322,30 @@
         )
         for i in range(1, ny)
     ]
-    for c in steps[0]:
-        c.start()
-    for chain in steps_left[0:1]:
+    for chain in steps[0:1] + steps_left[0:1]:
         for c in chain:
             c.start()
     for c in q_sends:
         c.start()
-    load_n.wait()
-    load_b.wait()
+    weights.start()
     share = Tp(nx, pw, pw_xs, pw_xr, pw_ds, pw_dr)
     share.start()
 
-    for s in range(1, rights + 1):
-        for c in steps[s - 1]:
-            c.wait_recv()
-        if s < rights:
-            for c in steps[s]:
-                c.start()
+    for s in range(1, max(rights, weights.last(1, 0), weights.last(1, 1)) + 1):
+        if s <= rights:
+            for c in steps[s - 1]:
+                c.wait_recv()
+            if s < rights:
+                for c in steps[s]:
+                    c.start()
         if s <= lefts:
             for c in steps_left[s - 1]:
                 c.wait_recv()
             if s < lefts:
                 for c in steps_left[s]:
                     c.start()
+        weights.step(s)
+    weights.lines()
 
     for r in range(nz):
         gk[:, r * tok : (r + 1) * tok] = jnp.where(r <= z, gbuf[r, :, 0:tok], FAR)
@@ -275,10 +398,20 @@
             c.start()
         return carry
 
-    lax.fori_loop(1, ny, one, 0)
+    tick = 0
+    ticks = weights.ticks()
+    cuts = [1, 4, 7, 8] if ny == 8 else [1, ny]
+    for a, b in zip(cuts[:-1], cuts[1:]):
+        lax.fori_loop(a, b, one, 0)
+        if tick < ticks:
+            weights.tick(tick)
+            tick += 1
     block(y, True, orecv.at[y], lrecv.at[y])
     for i in range(1, nx):
         share.forward(i)
+    if tick < ticks:
+        weights.tick(tick)
+        tick += 1
     for i in range(1, ny):
         for c in give(i):
             c.wait_recv()
@@ -305,24 +438,70 @@
         hand(i).start()
     arecv[tp] = asend[tp]
     share.finish()
+    if tick < ticks:
+        weights.tick(tick)
+        tick += 1
     for i in range(1, nt):
         hand(i).wait_recv()
 
     full = jnp.concatenate([arecv[t] for t in range(nt)], axis=1)
     projected = jnp.dot(full, pw[...].reshape(nt * 128, d), preferred_element_type=F32)
+    for c in load_r:
+        c.wait()
     mixed = (res[...].astype(F32) + projected).astype(BF)
-    mixed_out[...] = mixed
     wide = mixed.astype(F32)
     scale = lax.rsqrt(jnp.mean(wide * wide, axis=-1, keepdims=True) + 1e-6)
     feat[tp] = (wide * scale * gain[...]).astype(BF)
 
     spread = Tp(nx, feat, f_xs, f_xr, f_ds, f_dr)
     spread.start()
+    if tick < ticks:
+        weights.tick(tick)
+        tick += 1
     for i in range(1, nx):
         spread.forward(i)
+    while tick < ticks:
+        weights.tick(tick)
+        tick += 1
     spread.finish()
-    feat_out[...] = feat[...]
-
+
+    ff = up.shape[3]
+    h = jnp.dot(feat[...].reshape(nt * rows, d), up[...].reshape(d, ff), preferred_element_type=F32)
+    h = jnp.square(jnp.maximum(h, 0.0)).astype(BF)
+    total = nt_dot(h, down[...].reshape(d, ff))
+    for t in range(nt):
+        piece = total[t * rows : (t + 1) * rows]
+
+        @pl.when(core == t % 2)
+        def _():
+            part[t // 2] = piece
+
+        @pl.when(core != t % 2)
+        def _():
+            psum[t // 2] = piece.astype(BF)
+
+    beside = (sp, x * 2 + 1 - core)
+    swap = rcopy(psum, pair, pair_s, pair_r, beside)
+    swap.start()
+    swap.wait()
+
+    def spare(i):
+        to = (x + i) % nx
+        return rcopy(psum.at[to], got.at[i - 1], g_s.at[i - 1], g_r.at[i - 1], (sp, to * 2 + core))
+
+    for i in range(1, nx):
+        to = (x + i) % nx
+        psum[to] = (part[to] + pair[to].astype(F32)).astype(BF)
+        spare(i).start()
+    acc = wide + (part[x] + pair[x].astype(F32))
+    for i in range(1, nx):
+        spare(i).wait_recv()
+        acc = acc + got[i - 1].astype(F32)
+    out[...] = acc.astype(BF)
+
+    for i in range(1, nx):
+        spare(i).wait_send()
+    weights.finish()
     for chain in steps + steps_left:
         for c in chain:
             c.wait_send()
@@ -335,85 +514,28 @@
         hand(i).wait_send()
 
 
-def ffn(nt, feat, mixed, w, out, up, down, part, pair, psum, got, w_in, pair_s, pair_r, g_s, g_r):
-    nx = nt // 2
-    sp, tp = lax.axis_index("sp"), lax.axis_index("tp")
-    x, c = tp // 2, tp % 2
-    rows, d = mixed.shape
-    nsp, band = up.shape[0], up.shape[1]
-    load_up = pltpu.make_async_copy(w.at[:, 0:band], up, w_in.at[0])
-    load_down = pltpu.make_async_copy(w.at[:, band : 2 * band], down, w_in.at[1])
-    load_up.start()
-    load_down.start()
-
-    barrier = pltpu.get_barrier_semaphore()
-    beside = (sp, x * 2 + 1 - c)
-    peers = [beside] + [(sp, ((x + i) % nx) * 2 + c) for i in range(1, nx)]
-    for peer in peers:
-        pl.semaphore_signal(barrier, inc=1, device_id=peer, device_id_type=MESH)
-    pl.semaphore_wait(barrier, len(peers))
-
-    load_up.wait()
-    f = feat[...].reshape(nt * rows, d)
-    ff = up.shape[2]
-    h = jnp.dot(f, up[...].reshape(nsp * band, ff), preferred_element_type=F32)
-    h = jnp.square(jnp.maximum(h, 0.0)).astype(BF)
-    load_down.wait()
-    total = nt_dot(h, down[...].reshape(nsp * band, ff))
-    for t in range(nt):
-        block = total[t * rows : (t + 1) * rows]
-
-        @pl.when(c == t % 2)
-        def _():
-            part[t // 2] = block
-
-        @pl.when(c != t % 2)
-        def _():
-            psum[t // 2] = block.astype(BF)
-
-    swap = rcopy(psum, pair, pair_s, pair_r, beside)
-    swap.start()
-    swap.wait()
-
-    def give(i):
-        to = (x + i) % nx
-        return rcopy(psum.at[to], got.at[i - 1], g_s.at[i - 1], g_r.at[i - 1], (sp, to * 2 + c))
-
-    for i in range(1, nx):
-        to = (x + i) % nx
-        psum[to] = (part[to] + pair[to].astype(F32)).astype(BF)
-        give(i).start()
-    acc = mixed[...].astype(F32) + (part[x] + pair[x].astype(F32))
-    for i in range(1, nx):
-        give(i).wait_recv()
-        acc = acc + got[i - 1].astype(F32)
-    out[...] = acc.astype(BF)
-    for i in range(1, nx):
-        give(i).wait_send()
-
-
 def local(nz, ny, nt, *args):
     res, qn, kn, vn, qb, kb, vb, gn, gb, pn, pb, gain, up, down = args
     tok = qn.shape[0]
     rows, d = res.shape
     nx = nt // 2
     band, ff = up.shape
-    nsp = nz * ny
-    w = jnp.concatenate([up, down.T], axis=0)
-    w = lax.all_gather(w, "sp", axis=0, tiled=True).reshape(nsp, 2 * band, ff)
 
     dma = pltpu.SemaphoreType.DMA
-    vmem = pl.BlockSpec(memory_space=pltpu.VMEM)
     anyw = pl.BlockSpec(memory_space=pl.ANY)
-    mixed, feat = pl.pallas_call(
-        functools.partial(front, nz, ny, nt),
-        out_shape=(
-            jax.ShapeDtypeStruct((rows, d), BF),
-            jax.ShapeDtypeStruct((nt, rows, d), BF),
-        ),
-        in_specs=[vmem] * 8 + [anyw] * 2 + [vmem] * 2,
-        out_specs=(vmem, vmem),
+    return pl.pallas_call(
+        functools.partial(layer, nz, ny, nt),
+        out_shape=jax.ShapeDtypeStruct((rows, d), BF),
+        in_specs=[anyw] * 14,
+        out_specs=pl.BlockSpec(memory_space=pltpu.VMEM),
         scratch_shapes=[
+            pltpu.VMEM((6, 64, tok), BF),
+            pltpu.VMEM((2, tok), F32),
+            pltpu.VMEM((1, tok), F32),
+            pltpu.VMEM((rows, d), BF),
+            pltpu.VMEM((1, d), F32),
+            pltpu.VMEM((nz, ny, band, ff), BF),
+            pltpu.VMEM((nz, ny, band, ff), BF),
             pltpu.VMEM((ny, tok + 16, 128), BF),
             pltpu.VMEM((nz, tok, 128), BF),
             pltpu.VMEM((nz, tok, 256), BF),
@@ -427,7 +549,11 @@
             pltpu.VMEM((nt, rows, 128), BF),
             pltpu.VMEM((nt, rows, 128), BF),
             pltpu.VMEM((nt, rows, d), BF),
-            dma((2,)),
+            pltpu.VMEM((nx, rows, d), F32),
+            pltpu.VMEM((nx, rows, d), BF),
+            pltpu.VMEM((nx, rows, d), BF),
+            pltpu.VMEM((nx - 1, rows, d), BF),
+            dma((14,)),
             dma((ny - 1,)),
             dma((ny - 1,)),
             dma((3, nz - 1)),
@@ -444,42 +570,20 @@
             dma((nx - 1,)),
             dma((nx,)),
             dma((nx,)),
-        ],
-        compiler_params=pltpu.CompilerParams(
-            collective_id=0, has_side_effects=True, vmem_limit_bytes=48 * 1024 * 1024
-        ),
-        cost_estimate=pl.CostEstimate(
-            flops=8_000_000_000, bytes_accessed=60_000_000, transcendentals=7_000_000
-        ),
-        name="front",
-    )(qn, qb, kn, kb, vn, vb, gn, gb, pn, pb, res, gain.reshape(1, d))
-
-    return pl.pallas_call(
-        functools.partial(ffn, nt),
-        out_shape=jax.ShapeDtypeStruct((rows, d), BF),
-        in_specs=[vmem, vmem, anyw],
-        out_specs=vmem,
-        scratch_shapes=[
-            pltpu.VMEM((nsp, band, ff), BF),
-            pltpu.VMEM((nsp, band, ff), BF),
-            pltpu.VMEM((nx, rows, d), F32),
-            pltpu.VMEM((nx, rows, d), BF),
-            pltpu.VMEM((nx, rows, d), BF),
-            pltpu.VMEM((nx - 1, rows, d), BF),
-            dma((2,)),
+            dma((2, 2, max(ny, nz) // 2)),
+            dma((2, 2, max(ny, nz) // 2)),
+            dma((2, 2, max(ny, nz) // 2, 2)),
+            dma((2, 2, max(ny, nz) // 2, 2)),
             dma,
             dma,
             dma((nx - 1,)),
             dma((nx - 1,)),
         ],
         compiler_params=pltpu.CompilerParams(
-            collective_id=1, has_side_effects=True, vmem_limit_bytes=48 * 1024 * 1024
+            collective_id=0, has_side_effects=True, vmem_limit_bytes=64 * 1024 * 1024 - 65536
         ),
-        cost_estimate=pl.CostEstimate(
-            flops=1_600_000_000, bytes_accessed=20_000_000, transcendentals=0
-        ),
-        name="ffn",
-    )(feat, mixed, w)
+        name="layer",
+    )(qn.T, qb.T, kn.T, kb.T, vn.T, vb.T, gn.T, gb.T, pn, pb, res, gain.reshape(1, d), up, down.T)
 
 
 def solution(mesh):

time: 141 us -> 106 us (0.75)
  waiting for transfers between devices: 34 us -> 0 us
  Pallas kernels: 80.8 us -> 105 us
  between operations: 13.4 us -> 0.01 us
  local copies, waits for them, and re-layouts: 11 us -> 1.54 us
  other arithmetic: 1.52 us -> 0 us
    all_gather x1 -> x0, waiting for transfers between devices: 34 us -> none  [local(): w = lax.all_gather(w, 'sp', axis=0, tiled=True).reshape(nsp, 2 * band, ff)]
    pallas_call x2 -> x1, Pallas kernels: 80.8 us -> 105 us  [local(): pl.pallas_call(functools.partial(layer, nz, ny, nt), out_shape=jax.ShapeD...]
    unnamed x17 -> x1, local copies, waits for them, and re-layouts: 11 us -> 1.54 us
    concatenate x1 -> x0, other arithmetic: 1.52 us -> none  [local(): w = jnp.concatenate([up, down.T], axis=0)]
  transfers between devices with their start and end apart: 1 -> 0, of which waited for: 1 -> 0; matrix products, arithmetic and copies ran while one was open for 5% -> 0% of each run, Pallas kernels for 46% -> 0%
where the time goes in v2:
time: 106 us
  Pallas kernels  105 us (99%)
  local copies, waits for them, and re-layouts  1.54 us (1%)
    pallas_call x1, Pallas kernels, local(): pl.pallas_call(functools.partial(layer, nz, ny, nt), out_shape=jax.ShapeD...  105 us

profile of v2, /device:TPU:1, one launch (start us, length us, event | category | flops | bytes accessed | tf_op | source)
XLA Modules:
  0.0 106.1 jit_solution(17326758109629799403)
XLA Ops:
  0.0 104.5 %layer.1 = bf16[24,2048]{1,0:T(8,128)(2,1)} custom-call(bf16[64,192]{1,0:T(8,128)(2,1)} %bitcast.11, bf16[64,192]{1,0:T(8,128)(2,1)} %bitcast.12, bf16[64,192]{1,0:T(8,128)(2,1)} %bitcast.13, bf16[64,192]{1,0:T(8,128)(2,1)} %bitcast.14, bf16[64,192]{1,0:T(8,128)(2,1)} %bitcast.15, bf16[64,192]{1,0:T(8,128)(2,1)} %bitcast.16, f32[2,192]{1,0:T(2,128)} %bitcast.18, ...), custom_call_target="tpu_custom_call" | custom-call | tf_op jit(solution)/shard_map/layer/pallas_call | solution.py:526
  104.5 1.5 %copy.16 = bf16[24,2048]{1,0:T(8,128)(2,1)} copy(bf16[24,2048]{1,0:T(8,128)(2,1)} %layer.1) | data formatting | bytes 196608

commit v3 on v2

--- a/solution.py
+++ b/solution.py
@@ -87,93 +87,110 @@
 
 
 class Weights:
-    def __init__(self, nz, ny, up, down, s1, r1, s2, r2):
-        self.nz, self.ny = nz, ny
-        self.bufs = (up, down)
-        self.s1, self.r1, self.s2, self.r2 = s1, r1, s2, r2
+    def __init__(self, nz, ny, src, buf, d_s, d_r, w_s, w_r):
+        self.nz, self.ny, self.src, self.buf = nz, ny, src, buf
+        self.d_s, self.d_r, self.w_s, self.w_r = d_s, d_r, w_s, w_r
         self.sp, self.tp = lax.axis_index("sp"), lax.axis_index("tp")
         self.z, self.y = self.sp // ny, self.sp % ny
-
-    def shifted(self, along_y, by):
-        if along_y:
-            return self.z, (self.y + by + self.ny) % self.ny
-        return (self.z + by + self.nz) % self.nz, self.y
-
-    def length(self, along_y):
-        return self.ny if along_y else self.nz
-
-    def copy(self, phase, half, way, s, chunk, by):
-        along_y = (half == 0) == (phase == 1)
+        self.x, self.core = self.tp // 2, self.tp % 2
+        self.width = buf.shape[4]
+        self.mine = self.y % 2 == self.core
+        self.last = nz // 2
+
+    def half(self, c):
+        return pl.ds(pl.multiple_of(c * self.width, self.width), self.width)
+
+    def deal(self, t, c):
+        to_y = ((self.y // 2 + t) % (self.ny // 2)) * 2 + self.core
+        return rcopy(
+            self.src.at[:, :, self.half(c)],
+            self.buf.at[self.z, self.y],
+            self.d_s.at[t, c],
+            self.d_r.at[self.y],
+            (self.z * self.ny + to_y, self.x * 2 + c),
+        )
+
+    def start(self):
+        @pl.when(self.mine)
+        def _():
+            self.buf[self.z, self.y] = self.src[:, :, self.half(self.core)]
+
+        @pl.when(jnp.logical_not(self.mine))
+        def _():
+            self.deal(0, self.core).start()
+
+        self.deal(0, 1 - self.core).start()
+        n = self.ny // 2
+        for t in sorted(range(1, n), key=lambda t: min(t, n - t)):
+            for c in (0, 1):
+                self.deal(t, c).start()
+
+    def place(self, k):
+        far = (k + 1) // 2
+        return (self.y + far * (2 * (k % 2) - 1) + self.ny) % self.ny
+
+    def copy(self, way, s, k, by):
         sign = 1 - 2 * way
-        z, y = self.shifted(along_y, by)
-        buf = self.bufs[half]
-        if phase == 1:
-            ref = buf.at[z, y]
-            if s == self.length(along_y) // 2:
-                rows = buf.shape[2] // 2
-                ref = buf.at[z, y, way * rows : (way + 1) * rows]
-            send, recv = self.s1.at[half, way, s - 1], self.r1.at[half, way, s - 1]
+        ref = self.buf.at[(self.z - sign * by + self.nz) % self.nz, self.place(k)]
+        to = (self.z + sign + self.nz) % self.nz
+        return rcopy(
+            ref, ref, self.w_s.at[way, s - 1, k], self.w_r.at[way, s - 1, k], (to * self.ny + self.y, self.tp)
+        )
+
+    def ways(self, s, k):
+        return (k % 2,) if s == self.last else (0, 1)
+
+    def own(self, k):
+        def arrived():
+            at = self.place(k)
+            rcopy(
+                self.src.at[:, :, self.half(self.core)],
+                self.buf.at[self.z, at],
+                self.d_s.at[0, 0],
+                self.d_r.at[at],
+                (self.sp, self.x * 2 + 1 - self.core),
+            ).wait_recv()
+
+        if k == 0:
+            pl.when(jnp.logical_not(self.mine))(arrived)
         else:
-            if along_y:
-                part = self.nz // 2
-                ref = buf.at[chunk * part : (chunk + 1) * part, y]
-            else:
-                part = self.ny // 2
-                ref = buf.at[z, chunk * part : (chunk + 1) * part]
-            send, recv = self.s2.at[half, way, s - 1, chunk], self.r2.at[half, way, s - 1, chunk]
-        tz, ty = self.shifted(along_y, sign)
-        return rcopy(ref, ref, send, recv, (tz * self.ny + ty, self.tp))
-
-    def sent(self, phase, half, way, s, chunk=0):
-        return self.copy(phase, half, way, s, chunk, -(1 - 2 * way) * (s - 1))
-
-    def landed(self, phase, half, way, s, chunk=0):
-        return self.copy(phase, half, way, s, chunk, -(1 - 2 * way) * s)
-
-    def last(self, phase, half):
-        return self.length((half == 0) == (phase == 1)) // 2
-
-    def streams(self):
-        return [(half, way) for half in (0, 1) for way in (0, 1)]
-
-    def chunks(self, half, way, s):
-        return (way,) if s == self.last(2, half) else (0, 1)
-
-    def start(self):
-        for half, way in self.streams():
-            self.sent(1, half, way, 1).start()
-
-    def step(self, s):
-        for half, way in self.streams():
-            if s <= self.last(1, half):
-                self.landed(1, half, way, s).wait_recv()
-                if s < self.last(1, half):
-                    self.sent(1, half, way, s + 1).start()
-
-    def lines(self):
-        for chunk in (0, 1):
-            for half, way in self.streams():
-                if chunk in self.chunks(half, way, 1):
-                    self.sent(2, half, way, 1, chunk).start()
-
-    def tick(self, k):
-        s, chunk = k // 2 + 1, k % 2
-        for half, way in self.streams():
-            if s <= self.last(2, half) and chunk in self.chunks(half, way, s):
-                self.landed(2, half, way, s, chunk).wait_recv()
-                if s < self.last(2, half) and chunk in self.chunks(half, way, s + 1):
-                    self.sent(2, half, way, s + 1, chunk).start()
+            arrived()
+        for way in self.ways(1, k):
+            self.copy(way, 1, k, 0).start()
+
+    def tick(self, t):
+        s, k = t // self.ny + 1, t % self.ny
+        for way in self.ways(s, k):
+            self.copy(way, s, k, s).wait_recv()
+        if s < self.last:
+            for way in self.ways(s + 1, k):
+                self.copy(way, s + 1, k, s).start()
+
+    def tick_inner(self, t):
+        s, k = t // self.ny + 1, t % self.ny
+        for way in (0, 1):
+            self.copy(way, s, k, s).wait_recv()
+
+            @pl.when((s + 1 < self.last) | (k % 2 == way))
+            def _():
+                self.copy(way, s + 1, k, s).start()
 
     def ticks(self):
-        return 2 * max(self.last(2, 0), self.last(2, 1))
+        return self.last * self.ny
 
     def finish(self):
-        for half, way in self.streams():
-            for s in range(1, self.last(1, half) + 1):
-                self.sent(1, half, way, s).wait_send()
-            for s in range(1, self.last(2, half) + 1):
-                for chunk in self.chunks(half, way, s):
-                    self.sent(2, half, way, s, chunk).wait_send()
+        @pl.when(jnp.logical_not(self.mine))
+        def _():
+            self.deal(0, self.core).wait_send()
+
+        self.deal(0, 1 - self.core).wait_send()
+        for t in range(1, self.ny // 2):
+            for c in (0, 1):
+                self.deal(t, c).wait_send()
+        for s in range(1, self.last + 1):
+            for k in range(self.ny):
+                for way in self.ways(s, k):
+                    self.copy(way, s, k, s - 1).wait_send()
 
 
 def layer(
@@ -200,8 +217,8 @@
     graw_b,
     res,
     gain,
-    up,
-    down,
+    wsrc,
+    wbuf,
     qbuf,
     kbuf,
     vbuf,
@@ -218,7 +235,10 @@
     part,
     psum,
     pair,
+    xsend,
     got,
+    ysend,
+    yrecv,
     in_sem,
     q_s,
     q_r,
@@ -232,18 +252,22 @@
     p_r,
     a_s,
     a_r,
+    f_s,
+    f_r,
     f_xs,
     f_xr,
     f_ds,
     f_dr,
-    w_s1,
-    w_r1,
-    w_s2,
-    w_r2,
+    d_s,
+    d_r,
+    w_s,
+    w_r,
     pair_s,
     pair_r,
     g_s,
     g_r,
+    y_s,
+    y_r,
 ):
     nx = nt // 2
     sp, tp = lax.axis_index("sp"), lax.axis_index("tp")
@@ -256,6 +280,8 @@
     barrier = pltpu.get_barrier_semaphore()
     peers = [(z * ny + (y + i) % ny, tp) for i in range(1, ny)]
     up_z, down_z = ((z + 1) % nz) * ny + y, ((z + nz - 1) % nz) * ny + y
+    other = x * 2 + 1 - core
+    peers += [(z * ny + (y + i) % ny, other) for i in range(1, ny)]
     peers += [(up_z, tp), (down_z, tp)]
     peers += [(sp, (tp + i) % nt) for i in range(1, nt)]
     for peer in peers:
@@ -266,7 +292,7 @@
 
     loads = [load(i, r, raw.at[i]) for i, r in enumerate((qn, qb, kn, kb, vn, vb))]
     loads += [load(6, gn, graw_n), load(7, gb, graw_b)]
-    load_w = [load(8, up_in, up.at[z, y]), load(9, down_in, down.at[z, y])]
+    load_w = [load(8, up_in, wsrc.at[0]), load(9, down_in, wsrc.at[1])]
     load_p = [load(10, pn, pw.at[tp, 0:64]), load(11, pb, pw.at[tp, 64:128])]
     load_r = [load(12, res_in, res), load(13, gain_in, gain)]
     for c in loads + load_w + load_p + load_r:
@@ -296,7 +322,7 @@
         c.wait()
     pl.semaphore_wait(barrier, len(peers))
 
-    weights = Weights(nz, ny, up, down, w_s1, w_r1, w_s2, w_r2)
+    weights = Weights(nz, ny, wsrc, wbuf, d_s, d_r, w_s, w_r)
 
     def ring(slot, src, to):
         return [
@@ -316,22 +342,27 @@
     steps = [ring(s, s - 1, up_z) for s in range(1, rights + 1)]
     steps_left = [ring(nz - s, (nz - s + 1) % nz, down_z) for s in range(1, lefts + 1)]
 
-    q_sends = [
-        rcopy(
-            qbuf.at[y], qbuf.at[y], q_s.at[i - 1], q_r.at[i - 1], (z * ny + (y + i) % ny, tp)
+    def q_ring(way, s, by):
+        sign = 1 - 2 * way
+        ref = qbuf.at[(y - sign * by + ny) % ny]
+        return rcopy(
+            ref, ref, q_s.at[way, s - 1], q_r.at[way, s - 1], (z * ny + (y + sign + ny) % ny, tp)
         )
-        for i in range(1, ny)
-    ]
+
+    q_last = (ny // 2, ny - 1 - ny // 2)
     for chain in steps[0:1] + steps_left[0:1]:
         for c in chain:
             c.start()
-    for c in q_sends:
-        c.start()
+    for way in (0, 1):
+        if q_last[way] > 0:
+            q_ring(way, 1, 0).start()
     weights.start()
     share = Tp(nx, pw, pw_xs, pw_xr, pw_ds, pw_dr)
     share.start()
 
-    for s in range(1, max(rights, weights.last(1, 0), weights.last(1, 1)) + 1):
+    most = max(rights, q_last[0])
+    line = 0
+    for s in range(1, most + 1):
         if s <= rights:
             for c in steps[s - 1]:
                 c.wait_recv()
@@ -344,8 +375,14 @@
             if s < lefts:
                 for c in steps_left[s]:
                     c.start()
-        weights.step(s)
-    weights.lines()
+        for way in (0, 1):
+            if s <= q_last[way]:
+                q_ring(way, s, s).wait_recv()
+                if s < q_last[way]:
+                    q_ring(way, s + 1, s).start()
+        while line < ny * s // most:
+            weights.own(line)
+            line += 1
 
     for r in range(nz):
         gk[:, r * tok : (r + 1) * tok] = jnp.where(r <= z, gbuf[r, :, 0:tok], FAR)
@@ -392,26 +429,33 @@
 
     def one(i, carry):
         src = (y + ny - i) % ny
-        rcopy(qbuf.at[y], qbuf.at[src], q_s.at[i - 1], q_r.at[i - 1], (z * ny + src, tp)).wait_recv()
         block(src, False, osend.at[i - 1], lsend.at[i - 1])
         for c in give(i):
             c.start()
         return carry
 
-    tick = 0
     ticks = weights.ticks()
-    cuts = [1, 4, 7, 8] if ny == 8 else [1, ny]
-    for a, b in zip(cuts[:-1], cuts[1:]):
-        lax.fori_loop(a, b, one, 0)
-        if tick < ticks:
-            weights.tick(tick)
-            tick += 1
+    inner = max(0, ticks - ny)
+    per = min(2, inner // (ny - 1))
+
+    def paced(i, carry):
+        one(i, carry)
+        for j in range(per):
+            weights.tick_inner((i - 1) * per + j)
+        return carry
+
+    lax.fori_loop(1, ny, paced, 0)
+    todo = list(range(per * (ny - 1), ticks))
+
+    def go(count):
+        for t in todo[:count]:
+            weights.tick(t)
+        del todo[:count]
+
     block(y, True, orecv.at[y], lrecv.at[y])
     for i in range(1, nx):
         share.forward(i)
-    if tick < ticks:
-        weights.tick(tick)
-        tick += 1
+    go(3)
     for i in range(1, ny):
         for c in give(i):
             c.wait_recv()
@@ -438,9 +482,7 @@
         hand(i).start()
     arecv[tp] = asend[tp]
     share.finish()
-    if tick < ticks:
-        weights.tick(tick)
-        tick += 1
+    go(2)
     for i in range(1, nt):
         hand(i).wait_recv()
 
@@ -451,62 +493,87 @@
     mixed = (res[...].astype(F32) + projected).astype(BF)
     wide = mixed.astype(F32)
     scale = lax.rsqrt(jnp.mean(wide * wide, axis=-1, keepdims=True) + 1e-6)
-    feat[tp] = (wide * scale * gain[...]).astype(BF)
-
-    spread = Tp(nx, feat, f_xs, f_xr, f_ds, f_dr)
-    spread.start()
-    if tick < ticks:
-        weights.tick(tick)
-        tick += 1
+    half = y % 2
+    feat[half, tp] = (wide * scale * gain[...]).astype(BF)
+    partner = (z * ny + y + 1 - 2 * half, tp)
+    near = Tp(nx, feat.at[half], f_xs.at[0], f_xr.at[0], f_ds.at[0], f_dr.at[0])
+    far = Tp(nx, feat.at[1 - half], f_xs.at[1], f_xr.at[1], f_ds.at[1], f_dr.at[1])
+
+    def across_y(which):
+        return rcopy(feat.at[which, tp], feat.at[which, tp], f_s, f_r, partner)
+
+    across_y(half).start()
+    near.start()
+    go(2)
+    across_y(1 - half).wait_recv()
+    far.start()
+    go(2)
     for i in range(1, nx):
-        spread.forward(i)
-    while tick < ticks:
-        weights.tick(tick)
-        tick += 1
-    spread.finish()
-
-    ff = up.shape[3]
-    h = jnp.dot(feat[...].reshape(nt * rows, d), up[...].reshape(d, ff), preferred_element_type=F32)
+        near.forward(i)
+    go(2)
+    for i in range(1, nx):
+        far.forward(i)
+    go(len(todo))
+    near.finish()
+    far.finish()
+
+    count = 2 * nt * rows
+    ff = wbuf.shape[4]
+    h = jnp.dot(feat[...].reshape(count, d), wbuf[:, :, 0].reshape(d, ff), preferred_element_type=F32)
     h = jnp.square(jnp.maximum(h, 0.0)).astype(BF)
-    total = nt_dot(h, down[...].reshape(d, ff))
-    for t in range(nt):
-        piece = total[t * rows : (t + 1) * rows]
-
-        @pl.when(core == t % 2)
-        def _():
-            part[t // 2] = piece
-
-        @pl.when(core != t % 2)
-        def _():
-            psum[t // 2] = piece.astype(BF)
-
-    beside = (sp, x * 2 + 1 - core)
-    swap = rcopy(psum, pair, pair_s, pair_r, beside)
+    total = nt_dot(h, wbuf[:, :, 1].reshape(d, ff))
+    for g in range(2):
+        for t in range(nt):
+            at = (g * nt + t) * rows
+            piece = total[at : at + rows]
+
+            @pl.when(core == t % 2)
+            def _():
+                part[t // 2, g] = piece
+
+            @pl.when(core != t % 2)
+            def _():
+                psum[t // 2, g] = piece.astype(BF)
+
+    swap = rcopy(psum, pair, pair_s, pair_r, (sp, other))
     swap.start()
     swap.wait()
 
     def spare(i):
         to = (x + i) % nx
-        return rcopy(psum.at[to], got.at[i - 1], g_s.at[i - 1], g_r.at[i - 1], (sp, to * 2 + core))
+        return rcopy(xsend.at[i - 1], got.at[i - 1], g_s.at[i - 1], g_r.at[i - 1], (sp, to * 2 + core))
 
     for i in range(1, nx):
         to = (x + i) % nx
-        psum[to] = (part[to] + pair[to].astype(F32)).astype(BF)
+        xsend[i - 1] = (part[to] + pair[to].astype(F32)).astype(BF)
         spare(i).start()
-    acc = wide + (part[x] + pair[x].astype(F32))
     for i in range(1, nx):
         spare(i).wait_recv()
-        acc = acc + got[i - 1].astype(F32)
-    out[...] = acc.astype(BF)
-
+
+    def gathered(g):
+        acc = part[x, g] + pair[x, g].astype(F32)
+        for i in range(1, nx):
+            acc = acc + got[i - 1, g].astype(F32)
+        return acc
+
+    ysend[...] = gathered(1 - half).astype(BF)
+    back = rcopy(ysend, yrecv, y_s, y_r, partner)
+    back.start()
+    acc = wide + gathered(half)
+    back.wait_recv()
+    out[...] = (acc + yrecv[...].astype(F32)).astype(BF)
+
+    back.wait_send()
+    across_y(half).wait_send()
     for i in range(1, nx):
         spare(i).wait_send()
     weights.finish()
     for chain in steps + steps_left:
         for c in chain:
             c.wait_send()
-    for c in q_sends:
-        c.wait_send()
+    for way in (0, 1):
+        for s in range(1, q_last[way] + 1):
+            q_ring(way, s, s - 1).wait_send()
     for i in range(1, ny):
         for c in give(i):
             c.wait_send()
@@ -534,8 +601,8 @@
             pltpu.VMEM((1, tok), F32),
             pltpu.VMEM((rows, d), BF),
             pltpu.VMEM((1, d), F32),
-            pltpu.VMEM((nz, ny, band, ff), BF),
-            pltpu.VMEM((nz, ny, band, ff), BF),
+            pltpu.VMEM((2, band, ff), BF),
+            pltpu.VMEM((nz, ny, 2, band, ff // 2), BF),
             pltpu.VMEM((ny, tok + 16, 128), BF),
             pltpu.VMEM((nz, tok, 128), BF),
             pltpu.VMEM((nz, tok, 256), BF),
@@ -548,14 +615,17 @@
             pltpu.VMEM((ny, 8, 256), F32),
             pltpu.VMEM((nt, rows, 128), BF),
             pltpu.VMEM((nt, rows, 128), BF),
-            pltpu.VMEM((nt, rows, d), BF),
-            pltpu.VMEM((nx, rows, d), F32),
-            pltpu.VMEM((nx, rows, d), BF),
-            pltpu.VMEM((nx, rows, d), BF),
-            pltpu.VMEM((nx - 1, rows, d), BF),
+            pltpu.VMEM((2, nt, rows, d), BF),
+            pltpu.VMEM((nx, 2, rows, d), F32),
+            pltpu.VMEM((nx, 2, rows, d), BF),
+            pltpu.VMEM((nx, 2, rows, d), BF),
+            pltpu.VMEM((nx - 1, 2, rows, d), BF),
+            pltpu.VMEM((nx - 1, 2, rows, d), BF),
+            pltpu.VMEM((rows, d), BF),
+            pltpu.VMEM((rows, d), BF),
             dma((14,)),
-            dma((ny - 1,)),
-            dma((ny - 1,)),
+            dma((2, ny // 2)),
+            dma((2, ny // 2)),
             dma((3, nz - 1)),
             dma((3, nz - 1)),
             dma((nx - 1,)),
@@ -566,18 +636,22 @@
             dma((2, ny - 1)),
             dma((nt - 1,)),
             dma((nt - 1,)),
-            dma((nx - 1,)),
-            dma((nx - 1,)),
-            dma((nx,)),
-            dma((nx,)),
-            dma((2, 2, max(ny, nz) // 2)),
-            dma((2, 2, max(ny, nz) // 2)),
-            dma((2, 2, max(ny, nz) // 2, 2)),
-            dma((2, 2, max(ny, nz) // 2, 2)),
+            dma,
+            dma,
+            dma((2, nx - 1)),
+            dma((2, nx - 1)),
+            dma((2, nx)),
+            dma((2, nx)),
+            dma((ny // 2, 2)),
+            dma((ny,)),
+            dma((2, nz // 2, ny)),
+            dma((2, nz // 2, ny)),
             dma,
             dma,
             dma((nx - 1,)),
             dma((nx - 1,)),
+            dma,
+            dma,
         ],
         compiler_params=pltpu.CompilerParams(
             collective_id=0, has_side_effects=True, vmem_limit_bytes=64 * 1024 * 1024 - 65536

time: 106 us -> 99.7 us (0.941)
  Pallas kernels: 105 us -> 98 us
    pallas_call x1, Pallas kernels: 105 us -> 98 us  [local(): pl.pallas_call(functools.partial(layer, nz, ny, nt), out_shape=jax.ShapeD...]
where the time goes in v3:
time: 99.7 us; the launch traced here: 99.5 us
  Pallas kernels  98 us (98%)
  local copies, waits for them, and re-layouts  1.54 us (2%)
    pallas_call x1, Pallas kernels, local(): pl.pallas_call(functools.partial(layer, nz, ny, nt), out_shape=jax.ShapeD...  98 us

profile of v3, /device:TPU:1, one launch (start us, length us, event | category | flops | bytes accessed | tf_op | source)
XLA Modules:
  0.0 99.5 jit_solution(10199815588492553118)
XLA Ops:
  0.0 98.0 %layer.1 = bf16[24,2048]{1,0:T(8,128)(2,1)} custom-call(bf16[64,192]{1,0:T(8,128)(2,1)} %bitcast.11, bf16[64,192]{1,0:T(8,128)(2,1)} %bitcast.12, bf16[64,192]{1,0:T(8,128)(2,1)} %bitcast.13, bf16[64,192]{1,0:T(8,128)(2,1)} %bitcast.14, bf16[64,192]{1,0:T(8,128)(2,1)} %bitcast.15, bf16[64,192]{1,0:T(8,128)(2,1)} %bitcast.16, f32[2,192]{1,0:T(2,128)} %bitcast.18, ...), custom_call_target="tpu_custom_call" | custom-call | tf_op jit(solution)/shard_map/layer/pallas_call | solution.py:593
  98.0 1.5 %copy.16 = bf16[24,2048]{1,0:T(8,128)(2,1)} copy(bf16[24,2048]{1,0:T(8,128)(2,1)} %layer.1) | data formatting | bytes 196608

commit v4 on v3

--- a/solution.py
+++ b/solution.py
@@ -121,9 +121,13 @@
 
         self.deal(0, 1 - self.core).start()
         n = self.ny // 2
-        for t in sorted(range(1, n), key=lambda t: min(t, n - t)):
+        self.later = sorted(range(1, n), key=lambda t: min(t, n - t))
+
+    def deal_on(self):
+        for t in self.later[:1]:
             for c in (0, 1):
                 self.deal(t, c).start()
+        del self.later[:1]
 
     def place(self, k):
         far = (k + 1) // 2
@@ -140,23 +144,31 @@
     def ways(self, s, k):
         return (k % 2,) if s == self.last else (0, 1)
 
+    def own_arrived(self, k):
+        at = self.place(k)
+        rcopy(
+            self.src.at[:, :, self.half(self.core)],
+            self.buf.at[self.z, at],
+            self.d_s.at[0, 0],
+            self.d_r.at[at],
+            (self.sp, self.x * 2 + 1 - self.core),
+        ).wait_recv()
+
     def own(self, k):
-        def arrived():
-            at = self.place(k)
-            rcopy(
-                self.src.at[:, :, self.half(self.core)],
-                self.buf.at[self.z, at],
-                self.d_s.at[0, 0],
-                self.d_r.at[at],
-                (self.sp, self.x * 2 + 1 - self.core),
-            ).wait_recv()
-
         if k == 0:
-            pl.when(jnp.logical_not(self.mine))(arrived)
+            pl.when(jnp.logical_not(self.mine))(lambda: self.own_arrived(k))
         else:
-            arrived()
+            self.own_arrived(k)
         for way in self.ways(1, k):
             self.copy(way, 1, k, 0).start()
+
+    def own_inner(self, k):
+        self.own_arrived(k)
+        for way in (0, 1):
+
+            @pl.when((self.last > 1) | (k % 2 == way))
+            def _():
+                self.copy(way, 1, k, 0).start()
 
     def tick(self, t):
         s, k = t // self.ny + 1, t % self.ny
@@ -232,6 +244,7 @@
     asend,
     arecv,
     feat,
+    hidden,
     part,
     psum,
     pair,
@@ -350,9 +363,9 @@
         )
 
     q_last = (ny // 2, ny - 1 - ny // 2)
-    for chain in steps[0:1] + steps_left[0:1]:
-        for c in chain:
-            c.start()
+    for kind in (2, 0, 1):
+        for chain in steps[0:1] + steps_left[0:1]:
+            chain[kind].start()
     for way in (0, 1):
         if q_last[way] > 0:
             q_ring(way, 1, 0).start()
@@ -362,27 +375,25 @@
 
     most = max(rights, q_last[0])
     line = 0
+    early = min(2, ny)
     for s in range(1, most + 1):
-        if s <= rights:
-            for c in steps[s - 1]:
-                c.wait_recv()
-            if s < rights:
-                for c in steps[s]:
-                    c.start()
-        if s <= lefts:
-            for c in steps_left[s - 1]:
-                c.wait_recv()
-            if s < lefts:
-                for c in steps_left[s]:
-                    c.start()
-        for way in (0, 1):
-            if s <= q_last[way]:
-                q_ring(way, s, s).wait_recv()
-                if s < q_last[way]:
-                    q_ring(way, s + 1, s).start()
-        while line < ny * s // most:
-            weights.own(line)
-            line += 1
+        for kind in (2, 0, 1):
+            for chain, end in ((steps, rights), (steps_left, lefts)):
+                if s <= end:
+                    chain[s - 1][kind].wait_recv()
+                    if s < end:
+                        chain[s][kind].start()
+            if kind == 0:
+                for way in (0, 1):
+                    if s <= q_last[way]:
+                        q_ring(way, s, s).wait_recv()
+                        if s < q_last[way]:
+                            q_ring(way, s + 1, s).start()
+        weights.deal_on()
+        if s >= most - 1:
+            while line < (early if s == most else early // 2):
+                weights.own(line)
+                line += 1
 
     for r in range(nz):
         gk[:, r * tok : (r + 1) * tok] = jnp.where(r <= z, gbuf[r, :, 0:tok], FAR)
@@ -436,9 +447,15 @@
 
     ticks = weights.ticks()
     inner = max(0, ticks - ny)
-    per = min(2, inner // (ny - 1))
+    per = min(1, inner // (ny - 1))
 
     def paced(i, carry):
+        if early < ny:
+
+            @pl.when(i <= ny - early)
+            def _():
+                weights.own_inner(i + early - 1)
+
         one(i, carry)
         for j in range(per):
             weights.tick_inner((i - 1) * per + j)
@@ -455,7 +472,7 @@
     block(y, True, orecv.at[y], lrecv.at[y])
     for i in range(1, nx):
         share.forward(i)
-    go(3)
+    go(ny)
     for i in range(1, ny):
         for c in give(i):
             c.wait_recv()
@@ -482,7 +499,7 @@
         hand(i).start()
     arecv[tp] = asend[tp]
     share.finish()
-    go(2)
+    go(1)
     for i in range(1, nt):
         hand(i).wait_recv()
 
@@ -520,53 +537,87 @@
     count = 2 * nt * rows
     ff = wbuf.shape[4]
     h = jnp.dot(feat[...].reshape(count, d), wbuf[:, :, 0].reshape(d, ff), preferred_element_type=F32)
-    h = jnp.square(jnp.maximum(h, 0.0)).astype(BF)
-    total = nt_dot(h, wbuf[:, :, 1].reshape(d, ff))
-    for g in range(2):
+    hidden[...] = jnp.square(jnp.maximum(h, 0.0)).astype(BF).reshape(2, nt * rows, ff)
+    away = 1 - half
+
+    def swap(g):
+        return rcopy(psum.at[g], pair.at[g], pair_s.at[g], pair_r.at[g], (sp, other))
+
+    for g in (away, half):
+        total = nt_dot(hidden[g], wbuf[:, :, 1].reshape(d, ff))
         for t in range(nt):
-            at = (g * nt + t) * rows
-            piece = total[at : at + rows]
+            piece = total[t * rows : (t + 1) * rows]
 
             @pl.when(core == t % 2)
             def _():
-                part[t // 2, g] = piece
+                part[g, t // 2] = piece
 
             @pl.when(core != t % 2)
             def _():
-                psum[t // 2, g] = piece.astype(BF)
-
-    swap = rcopy(psum, pair, pair_s, pair_r, (sp, other))
-    swap.start()
-    swap.wait()
-
-    def spare(i):
+                psum[g, t // 2] = piece.astype(BF)
+
+        swap(g).start()
+
+    def both(g, to):
+        return part[g, to] + pair[g, to].astype(F32)
+
+    opposite = nx // 2 if nx > 2 else 0
+    direct = [i for i in range(1, nx) if i != opposite]
+
+    def spare(which, i):
         to = (x + i) % nx
-        return rcopy(xsend.at[i - 1], got.at[i - 1], g_s.at[i - 1], g_r.at[i - 1], (sp, to * 2 + core))
-
-    for i in range(1, nx):
-        to = (x + i) % nx
-        xsend[i - 1] = (part[to] + pair[to].astype(F32)).astype(BF)
-        spare(i).start()
-    for i in range(1, nx):
-        spare(i).wait_recv()
-
-    def gathered(g):
-        acc = part[x, g] + pair[x, g].astype(F32)
-        for i in range(1, nx):
-            acc = acc + got[i - 1, g].astype(F32)
-        return acc
-
-    ysend[...] = gathered(1 - half).astype(BF)
-    back = rcopy(ysend, yrecv, y_s, y_r, partner)
-    back.start()
-    acc = wide + gathered(half)
-    back.wait_recv()
-    out[...] = (acc + yrecv[...].astype(F32)).astype(BF)
-
-    back.wait_send()
+        return rcopy(
+            xsend.at[which, i - 1],
+            got.at[which, i - 1],
+            g_s.at[which, i - 1],
+            g_r.at[which, i - 1],
+            (sp, to * 2 + core),
+        )
+
+    def over(j):
+        return rcopy(ysend.at[j], yrecv.at[j], y_s.at[j], y_r.at[j], partner)
+
+    swap(away).wait_recv()
+    if opposite:
+        ysend[1] = both(away, (x + opposite) % nx).astype(BF)
+        over(1).start()
+    for i in direct:
+        xsend[0, i - 1] = both(away, (x + i) % nx).astype(BF)
+        spare(0, i).start()
+    swap(half).wait_recv()
+    for i in direct:
+        xsend[1, i - 1] = both(half, (x + i) % nx).astype(BF)
+        spare(1, i).start()
+    if opposite:
+        over(1).wait_recv()
+        xsend[1, opposite - 1] = (both(half, (x + opposite) % nx) + yrecv[1].astype(F32)).astype(BF)
+        spare(1, opposite).start()
+    acc = both(away, x)
+    for i in direct:
+        spare(0, i).wait_recv()
+        acc = acc + got[0, i - 1].astype(F32)
+    ysend[0] = acc.astype(BF)
+    over(0).start()
+    acc = wide + both(half, x)
+    for i in direct:
+        spare(1, i).wait_recv()
+        acc = acc + got[1, i - 1].astype(F32)
+    if opposite:
+        spare(1, opposite).wait_recv()
+        acc = acc + got[1, opposite - 1].astype(F32)
+    over(0).wait_recv()
+    out[...] = (acc + yrecv[0].astype(F32)).astype(BF)
+
+    over(0).wait_send()
+    if opposite:
+        over(1).wait_send()
+        spare(1, opposite).wait_send()
+    for g in range(2):
+        swap(g).wait_send()
     across_y(half).wait_send()
-    for i in range(1, nx):
-        spare(i).wait_send()
+    for i in direct:
+        for which in (0, 1):
+            spare(which, i).wait_send()
     weights.finish()
     for chain in steps + steps_left:
         for c in chain:
@@ -616,13 +667,14 @@
             pltpu.VMEM((nt, rows, 128), BF),
             pltpu.VMEM((nt, rows, 128), BF),
             pltpu.VMEM((2, nt, rows, d), BF),
-            pltpu.VMEM((nx, 2, rows, d), F32),
-            pltpu.VMEM((nx, 2, rows, d), BF),
-            pltpu.VMEM((nx, 2, rows, d), BF),
-            pltpu.VMEM((nx - 1, 2, rows, d), BF),
-            pltpu.VMEM((nx - 1, 2, rows, d), BF),
-            pltpu.VMEM((rows, d), BF),
-            pltpu.VMEM((rows, d), BF),
+            pltpu.VMEM((2, nt * rows, ff // 2), BF),
+            pltpu.VMEM((2, nx, rows, d), F32),
+            pltpu.VMEM((2, nx, rows, d), BF),
+            pltpu.VMEM((2, nx, rows, d), BF),
+            pltpu.VMEM((2, nx - 1, rows, d), BF),
+            pltpu.VMEM((2, nx - 1, rows, d), BF),
+            pltpu.VMEM((2, rows, d), BF),
+            pltpu.VMEM((2, rows, d), BF),
             dma((14,)),
             dma((2, ny // 2)),
             dma((2, ny // 2)),
@@ -646,12 +698,12 @@
             dma((ny,)),
             dma((2, nz // 2, ny)),
             dma((2, nz // 2, ny)),
-            dma,
-            dma,
-            dma((nx - 1,)),
-            dma((nx - 1,)),
-            dma,
-            dma,
+            dma((2,)),
+            dma((2,)),
+            dma((2, nx - 1)),
+            dma((2, nx - 1)),
+            dma((2,)),
+            dma((2,)),
         ],
         compiler_params=pltpu.CompilerParams(
             collective_id=0, has_side_effects=True, vmem_limit_bytes=64 * 1024 * 1024 - 65536

time: 99.7 us -> 96.1 us (0.964)
  Pallas kernels: 98 us -> 94.4 us
    pallas_call x1, Pallas kernels: 98 us -> 94.4 us  [local(): pl.pallas_call(functools.partial(layer, nz, ny, nt), out_shape=jax.ShapeD...]
where the time goes in v4:
time: 96.1 us; the launch traced here: 96 us
  Pallas kernels  94.4 us (98%)
  local copies, waits for them, and re-layouts  1.54 us (2%)
    pallas_call x1, Pallas kernels, local(): pl.pallas_call(functools.partial(layer, nz, ny, nt), out_shape=jax.ShapeD...  94.4 us

profile of v4, /device:TPU:1, one launch (start us, length us, event | category | flops | bytes accessed | tf_op | source)
XLA Modules:
  0.0 96.0 jit_solution(16113931704177670759)
XLA Ops:
  0.0 94.4 %layer.1 = bf16[24,2048]{1,0:T(8,128)(2,1)} custom-call(bf16[64,192]{1,0:T(8,128)(2,1)} %bitcast.11, bf16[64,192]{1,0:T(8,128)(2,1)} %bitcast.12, bf16[64,192]{1,0:T(8,128)(2,1)} %bitcast.13, bf16[64,192]{1,0:T(8,128)(2,1)} %bitcast.14, bf16[64,192]{1,0:T(8,128)(2,1)} %bitcast.15, bf16[64,192]{1,0:T(8,128)(2,1)} %bitcast.16, f32[2,192]{1,0:T(2,128)} %bitcast.18, ...), custom_call_target="tpu_custom_call" | custom-call | tf_op jit(solution)/shard_map/layer/pallas_call | solution.py:644
  94.4 1.5 %copy.16 = bf16[24,2048]{1,0:T(8,128)(2,1)} copy(bf16[24,2048]{1,0:T(8,128)(2,1)} %layer.1) | data formatting | bytes 196608

commit v5 on v4

--- a/solution.py
+++ b/solution.py
@@ -121,7 +121,13 @@
 
         self.deal(0, 1 - self.core).start()
         n = self.ny // 2
-        self.later = sorted(range(1, n), key=lambda t: min(t, n - t))
+        self.later = []
+        for t in range(1, n // 2 + 1):
+            if 2 * t == n:
+                self.later.append(t)
+            else:
+                self.later += [t + self.core * (n - 2 * t), n - t - self.core * (n - 2 * t)]
+        self.deal_on()
 
     def deal_on(self):
         for t in self.later[:1]:
@@ -375,7 +381,7 @@
 
     most = max(rights, q_last[0])
     line = 0
-    early = min(2, ny)
+    early = min(4, ny)
     for s in range(1, most + 1):
         for kind in (2, 0, 1):
             for chain, end in ((steps, rights), (steps_left, lefts)):
@@ -390,10 +396,9 @@
                         if s < q_last[way]:
                             q_ring(way, s + 1, s).start()
         weights.deal_on()
-        if s >= most - 1:
-            while line < (early if s == most else early // 2):
-                weights.own(line)
-                line += 1
+        if line < early:
+            weights.own(line)
+            line += 1
 
     for r in range(nz):
         gk[:, r * tok : (r + 1) * tok] = jnp.where(r <= z, gbuf[r, :, 0:tok], FAR)
@@ -472,10 +477,12 @@
     block(y, True, orecv.at[y], lrecv.at[y])
     for i in range(1, nx):
         share.forward(i)
-    go(ny)
+    go(3)
     for i in range(1, ny):
         for c in give(i):
             c.wait_recv()
+
+    go(4)
 
     lse = [lrecv[j, :, 0:tok] for j in range(ny)]
     peak = functools.reduce(jnp.maximum, lse)
@@ -498,8 +505,8 @@
     for i in range(1, nt):
         hand(i).start()
     arecv[tp] = asend[tp]
+    go(3)
     share.finish()
-    go(1)
     for i in range(1, nt):
         hand(i).wait_recv()
 
@@ -521,13 +528,13 @@
 
     across_y(half).start()
     near.start()
-    go(2)
+    go(4)
     across_y(1 - half).wait_recv()
     far.start()
-    go(2)
+    go(3)
     for i in range(1, nx):
         near.forward(i)
-    go(2)
+    go(3)
     for i in range(1, nx):
         far.forward(i)
     go(len(todo))

time: 96.1 us -> 90 us (0.937)
  Pallas kernels: 94.4 us -> 88.2 us
    pallas_call x1, Pallas kernels: 94.4 us -> 88.2 us  [local(): pl.pallas_call(functools.partial(layer, nz, ny, nt), out_shape=jax.ShapeD...]
where the time goes in v5:
time: 90 us; the launch traced here: 89.8 us
  Pallas kernels  88.2 us (98%)
  local copies, waits for them, and re-layouts  1.54 us (2%)
    pallas_call x1, Pallas kernels, local(): pl.pallas_call(functools.partial(layer, nz, ny, nt), out_shape=jax.ShapeD...  88.2 us

profile of v5, /device:TPU:1, one launch (start us, length us, event | category | flops | bytes accessed | tf_op | source)
XLA Modules:
  0.0 89.8 jit_solution(12773347967750712420)
XLA Ops:
  0.0 88.2 %layer.1 = bf16[24,2048]{1,0:T(8,128)(2,1)} custom-call(bf16[64,192]{1,0:T(8,128)(2,1)} %bitcast.11, bf16[64,192]{1,0:T(8,128)(2,1)} %bitcast.12, bf16[64,192]{1,0:T(8,128)(2,1)} %bitcast.13, bf16[64,192]{1,0:T(8,128)(2,1)} %bitcast.14, bf16[64,192]{1,0:T(8,128)(2,1)} %bitcast.15, bf16[64,192]{1,0:T(8,128)(2,1)} %bitcast.16, f32[2,192]{1,0:T(2,128)} %bitcast.18, ...), custom_call_target="tpu_custom_call" | custom-call | tf_op jit(solution)/shard_map/layer/pallas_call | solution.py:651
  88.2 1.5 %copy.16 = bf16[24,2048]{1,0:T(8,128)(2,1)} copy(bf16[24,2048]{1,0:T(8,128)(2,1)} %layer.1) | data formatting | bytes 196608

commit v6 on v5

--- a/solution.py
+++ b/solution.py
@@ -382,6 +382,8 @@
     most = max(rights, q_last[0])
     line = 0
     early = min(4, ny)
+    weights.own(0)
+    line = 1
     for s in range(1, most + 1):
         for kind in (2, 0, 1):
             for chain, end in ((steps, rights), (steps_left, lefts)):

time: 90 us -> 88.8 us (0.987)
  Pallas kernels: 88.2 us -> 87.1 us
    pallas_call x1, Pallas kernels: 88.2 us -> 87.1 us  [local(): pl.pallas_call(functools.partial(layer, nz, ny, nt), out_shape=jax.ShapeD...]
where the time goes in v6:
time: 88.8 us; the launch traced here: 88.7 us
  Pallas kernels  87.1 us (98%)
  local copies, waits for them, and re-layouts  1.54 us (2%)
    pallas_call x1, Pallas kernels, local(): pl.pallas_call(functools.partial(layer, nz, ny, nt), out_shape=jax.ShapeD...  87.1 us

profile of v6, /device:TPU:1, one launch (start us, length us, event | category | flops | bytes accessed | tf_op | source)
XLA Modules:
  0.0 88.7 jit_solution(13236991125278341785)
XLA Ops:
  0.0 87.1 %layer.1 = bf16[24,2048]{1,0:T(8,128)(2,1)} custom-call(bf16[64,192]{1,0:T(8,128)(2,1)} %bitcast.11, bf16[64,192]{1,0:T(8,128)(2,1)} %bitcast.12, bf16[64,192]{1,0:T(8,128)(2,1)} %bitcast.13, bf16[64,192]{1,0:T(8,128)(2,1)} %bitcast.14, bf16[64,192]{1,0:T(8,128)(2,1)} %bitcast.15, bf16[64,192]{1,0:T(8,128)(2,1)} %bitcast.16, f32[2,192]{1,0:T(2,128)} %bitcast.18, ...), custom_call_target="tpu_custom_call" | custom-call | tf_op jit(solution)/shard_map/layer/pallas_call | solution.py:653
  87.1 1.5 %copy.16 = bf16[24,2048]{1,0:T(8,128)(2,1)} copy(bf16[24,2048]{1,0:T(8,128)(2,1)} %layer.1) | data formatting | bytes 196608
